TPU v7x, 128 devices: a whole 4x4x4 slice. The times are simulated.
128 devices in a mesh: dp: 4 (over x), kv: 16 (over z, y), tp: 2 (over core).
Axes of the slice: x: 4, y: 4, z: 4, core: 2. Of those that a mesh axis runs over, the one named last changes fastest.
Arguments:
- tokens: bfloat16 [512, 2048], P('dp', ('kv', 'tp')), may hold values from -60 to 60
- first_norm_gain: float32 [2048], replicated, may hold values from 0.1 to 1.9
- first_gate_weight: bfloat16 [2048, 5632], P(None, ('kv', 'tp')), may hold values from -0.125 to 0.125
- first_up_weight: bfloat16 [2048, 5632], P(None, ('kv', 'tp')), may hold values from -0.125 to 0.125
- first_down_weight: bfloat16 [5632, 2048], P(('kv', 'tp')), may hold values from -0.15625 to 0.15625
- mixer_norm_gain: float32 [2048], replicated, may hold values from 0.1 to 1.9
- query_weight: bfloat16 [2048, 1024], P('kv', 'tp'), may hold values from -0.125 to 0.125
- key_weight: bfloat16 [2048, 1024], P('kv', 'tp'), may hold values from -0.125 to 0.125
- value_weight: bfloat16 [2048, 1024], P('kv', 'tp'), may hold values from -0.125 to 0.125
- output_gate_weight: bfloat16 [2048, 1024], P('kv', 'tp'), may hold values from -0.125 to 0.125
- strength_weight: bfloat16 [2048, 8], replicated, may hold values from -0.125 to 0.125
- decay_weight: bfloat16 [2048, 8], replicated, may hold values from -0.125 to 0.125
- head_decay_log: float32 [8], replicated, may hold values from 0 to 2.77
- decay_input_bias: float32 [8], replicated, may hold values from -4 to 0
- decay_extra_log: float32 [512, 8], P(('dp', 'kv'), 'tp'), may hold values from -0.7 to 0
- head_norm_gain: float32 [128], replicated, may hold values from 0.1 to 1.9
- state: float32 [512, 8, 128, 128], P(('dp', 'kv'), 'tp'), may hold values from -0.6 to 0.6
- mixer_output_weight: bfloat16 [1024, 2048], P('tp', 'kv'), may hold values from -0.1875 to 0.1875
- second_norm_gain: float32 [2048], replicated, may hold values from 0.1 to 1.9
- second_gate_weight: bfloat16 [2048, 5632], P(None, ('kv', 'tp')), may hold values from -0.125 to 0.125
- second_up_weight: bfloat16 [2048, 5632], P(None, ('kv', 'tp')), may hold values from -0.125 to 0.125
- second_down_weight: bfloat16 [5632, 2048], P(('kv', 'tp')), may hold values from -0.15625 to 0.15625
Outputs:
- layer_out: bfloat16 [512, 2048], P('dp', ('kv', 'tp'))
- new_state: float32 [512, 8, 128, 128], P(('dp', 'kv'), 'tp')
All inputs are finite; a program needn't handle non-finite values.
Results may differ from a plain program's by a relative error of at most 0.014.
Values may be sent and summed in bfloat16 or wider, within the bound.
A program may use at most 64 MiB of HBM per device.

v0:
```python
import jax
import jax.numpy as jnp
from jax import lax
from jax.sharding import PartitionSpec as P

EPS = 1e-06


def from_everyone(shard, axis):
    size = lax.axis_size(axis)
    return lax.all_to_all(
        jnp.broadcast_to(shard[None], (size, *shard.shape)), axis, 0, 0, tiled=True
    )


def laid_out(tiles, dim):
    tiles = jnp.moveaxis(tiles, 0, dim)
    lengths = tiles.shape
    return tiles.reshape(*lengths[:dim], lengths[dim] * lengths[dim + 1], *lengths[dim + 2 :])


def gathered_copies(shard, axis, dim):
    tiles = from_everyone(shard, axis)
    return laid_out(tiles, dim)


def split_up(shard, dim, size):
    before, after = (shard.shape[:dim], shard.shape[dim + 1 :])
    return jnp.moveaxis(shard.reshape(*before, size, -1, *after), dim, 0)


def sent_and_summed(shard, axis, dim):
    size = lax.axis_size(axis)
    tiles = lax.all_to_all(split_up(shard, dim, size), axis, 0, 0, tiled=True)
    return jnp.sum(tiles.astype(jnp.float32), axis=0)


def row_scale(values):
    return lax.rsqrt(jnp.mean(values * values, axis=-1, keepdims=True) + EPS)


def unit_rows(values):
    return values * lax.rsqrt(jnp.sum(values * values, axis=-1, keepdims=True) + EPS)


def block_terms(row_data, gain_vec, w_gate, w_up, w_down):
    rows32 = row_data.astype(jnp.float32)
    normed = (rows32 * row_scale(rows32) * gain_vec).astype(jnp.bfloat16)
    gate_pre = jnp.dot(normed, w_gate, preferred_element_type=jnp.float32)
    upward = jnp.dot(normed, w_up, preferred_element_type=jnp.float32)
    hidden = (jax.nn.silu(gate_pre) * upward).astype(jnp.bfloat16)
    return jnp.dot(hidden, w_down, preferred_element_type=jnp.float32)


def delta_step(
    query_vec, key_vec, value_vec, gate_vals, beta_gate, head_decay_rate, state, head_norm_gain
):
    recalled = jnp.einsum("shd,shde->she", key_vec, state)
    correction = beta_gate[..., None] * (value_vec - head_decay_rate[..., None] * recalled)
    new_state = (
        head_decay_rate[..., None, None] * state + key_vec[..., :, None] * correction[..., None, :]
    )
    read_out = jnp.einsum("shd,shde->she", query_vec, new_state)
    normed = read_out * row_scale(read_out) * head_norm_gain
    return (normed * jax.nn.silu(gate_vals), new_state)


def shards(
    tokens,
    first_norm_gain,
    first_gate_weight,
    first_up_weight,
    first_down_weight,
    mixer_norm_gain,
    query_weight,
    key_weight,
    value_weight,
    output_gate_weight,
    strength_weight,
    decay_weight,
    head_decay_log,
    decay_input_bias,
    decay_extra_log,
    head_norm_gain,
    state,
    mixer_output_weight,
    second_norm_gain,
    second_gate_weight,
    second_up_weight,
    second_down_weight,
):
    kv_index = lax.axis_index("kv")
    tp_index = lax.axis_index("tp")
    seq_dev, heads_dev, head_size = (state.shape[0], state.shape[1], state.shape[2])
    kv_width = query_weight.shape[0]
    head_cols = heads_dev * head_size
    rows_all = gathered_copies(tokens, ("kv", "tp"), 1)
    ffn_terms = block_terms(
        rows_all, first_norm_gain, first_gate_weight, first_up_weight, first_down_weight
    )
    whole_rows = None
    share_sum = sent_and_summed(ffn_terms.astype(jnp.bfloat16), ("kv", "tp"), 1)
    first_rows = (tokens.astype(jnp.float32) + 0.5 * share_sum).astype(jnp.bfloat16)
    first32 = first_rows.astype(jnp.float32)
    whole_rows = gathered_copies(first_rows, ("kv", "tp"), 1)
    whole32 = whole_rows.astype(jnp.float32)
    row_factor = row_scale(whole32)[:, 0]
    whole_scaled = (whole32 * mixer_norm_gain).astype(jnp.bfloat16)
    beta_pre = jnp.dot(whole_scaled, strength_weight, preferred_element_type=jnp.float32)
    decay_logits = jnp.dot(whole_scaled, decay_weight, preferred_element_type=jnp.float32)
    block_scaled = lax.dynamic_slice_in_dim(whole_scaled, kv_index * kv_width, kv_width, 1)
    projected = sent_and_summed(
        jnp.concatenate(
            [
                jnp.dot(block_scaled, weight, preferred_element_type=jnp.float32)
                for weight in (query_weight, key_weight, value_weight, output_gate_weight)
            ],
            axis=1,
        ).astype(jnp.bfloat16),
        "kv",
        0,
    )
    own_rows = kv_index * seq_dev
    own_factor = lax.dynamic_slice_in_dim(row_factor, own_rows, seq_dev)[:, None]
    projected = projected * own_factor

    def split_heads(role_index):
        return projected[:, role_index * head_cols : (role_index + 1) * head_cols].reshape(
            seq_dev, heads_dev, head_size
        )

    query_vec = unit_rows(jax.nn.silu(split_heads(0))) * head_size ** (-0.5)
    key_vec = unit_rows(jax.nn.silu(split_heads(1)))
    value_vec = jax.nn.silu(split_heads(2))
    gate_vals = split_heads(3)
    head_start = tp_index * heads_dev

    def local_gate_values(values):
        own_seqs = lax.dynamic_slice_in_dim(values, own_rows, seq_dev, 0)
        return lax.dynamic_slice_in_dim(own_seqs, head_start, heads_dev, 1) * own_factor

    beta_gate = jax.nn.sigmoid(local_gate_values(beta_pre))
    decay_log_term = lax.dynamic_slice_in_dim(head_decay_log, head_start, heads_dev)
    decay_offset_term = lax.dynamic_slice_in_dim(decay_input_bias, head_start, heads_dev)
    head_decay_rate = jnp.exp(
        decay_extra_log
        - jnp.exp(decay_log_term)
        * jax.nn.softplus(local_gate_values(decay_logits) + decay_offset_term)
    )
    heads_f32, new_state = delta_step(
        query_vec, key_vec, value_vec, gate_vals, beta_gate, head_decay_rate, state, head_norm_gain
    )
    heads_out = heads_f32.reshape(seq_dev, head_cols).astype(jnp.bfloat16)
    mixer_terms = jnp.dot(
        gathered_copies(heads_out, "kv", 0), mixer_output_weight, preferred_element_type=jnp.float32
    )
    mixer_sum = sent_and_summed(mixer_terms.astype(jnp.bfloat16), "tp", 1)
    second_rows = (first32 + mixer_sum).astype(jnp.bfloat16)
    rows_last = gathered_copies(second_rows, ("kv", "tp"), 1)
    last_terms = block_terms(
        rows_last, second_norm_gain, second_gate_weight, second_up_weight, second_down_weight
    )
    last_sum = sent_and_summed(last_terms.astype(jnp.bfloat16), ("kv", "tp"), 1)
    layer_out = (second_rows.astype(jnp.float32) + 0.5 * last_sum).astype(jnp.bfloat16)
    return (layer_out, new_state)


def solution(mesh):
    placed = (
        P("dp", ("kv", "tp")),
        P(),
        P(None, ("kv", "tp")),
        P(None, ("kv", "tp")),
        P(("kv", "tp"), None),
        P(),
        P("kv", "tp"),
        P("kv", "tp"),
        P("kv", "tp"),
        P("kv", "tp"),
        P(),
        P(),
        P(),
        P(),
        P(("dp", "kv"), "tp"),
        P(),
        P(("dp", "kv"), "tp", None, None),
        P("tp", "kv"),
        P(),
        P(None, ("kv", "tp")),
        P(None, ("kv", "tp")),
        P(("kv", "tp"), None),
    )
    return jax.shard_map(
        shards,
        mesh=mesh,
        in_specs=placed,
        out_specs=(P("dp", ("kv", "tp")), P(("dp", "kv"), "tp", None, None)),
        check_vma=False,
    )
```

profile of v0, /device:TPU:1, one launch (start us, length us, event | category | flops | bytes accessed | tf_op | source)
XLA Modules:
  0.0 126.3 jit_solution(17952828371805145332)
XLA Ops:
  0.7 0.9 broadcast_in_dim.8
  1.6 21.0 %all_to_all.40 = bf16[32,128,64]{1,2,0:T(8,128)(2,1)S(1)} all-to-all(bf16[32,128,64]{1,2,0:T(8,128)(2,1)S(1)} %broadcast_in_dim.8), channel_id=1, replica_groups=mesh['dp'=4,'kv'=16,'tp'=2] {'kv','tp'}, dimensions={0} | all-to-all | bytes 1048576 | tf_op jit(solution)/shard_map/all_to_all | solution.py:11
  22.6 0.3 multiply_reduce_fusion.2
  22.9 0.3 fusion.10
  23.2 0.3 fusion.50
  23.6 0.7 convolution_convert_fusion.1
  24.3 0.3 copy.30
  24.6 15.1 %all_to_all.41 = bf16[32,128,64]{1,2,0:T(8,128)(2,1)S(1)} all-to-all(bf16[32,128,64]{1,2,0:T(8,128)(2,1)S(1)} %bitcast.116), channel_id=1, replica_groups=mesh['dp'=4,'kv'=16,'tp'=2] {'kv','tp'}, dimensions={0} | all-to-all | bytes 1048576 | tf_op jit(solution)/shard_map/all_to_all | solution.py:34
  39.8 0.9 broadcast_in_dim.9
  40.7 3.9 %all-to-all-start.2 = ((bf16[32,128,64]{1,2,0:T(8,128)(2,1)}), bf16[32,128,64]{1,2,0:T(8,128)(2,1)S(1)}, u32[]{:S(2)}, u32[]{:S(2)}) async-start(bf16[32,128,64]{1,2,0:T(8,128)(2,1)} %broadcast_in_dim.9), calls=%async_computation.2 | async-start | bytes 1048576 | tf_op jit(solution)/shard_map/all_to_all | solution.py:11
  44.8 11.4 %all-to-all-done.2 = bf16[32,128,64]{1,2,0:T(8,128)(2,1)S(1)} async-done(((bf16[32,128,64]{1,2,0:T(8,128)(2,1)}), bf16[32,128,64]{1,2,0:T(8,128)(2,1)S(1)}, u32[]{:S(2)}, u32[]{:S(2)}) %all-to-all-start.2) | async-done | bytes 524320 | tf_op jit(solution)/shard_map/all_to_all | solution.py:11
  56.2 0.3 fusion.8
  56.7 0.2 fusion.1
  57.7 0.8 pad_maximum_fusion
  58.5 4.2 %all-to-all-start.3 = ((bf16[16,8,2048]{2,1,0:T(8,128)(2,1)}), bf16[16,8,2048]{2,1,0:T(8,128)(2,1)}, u32[]{:S(2)}, u32[]{:S(2)}) async-start(bf16[16,8,2048]{2,1,0:T(8,128)(2,1)} %pad_maximum_fusion), calls=%async_computation.3 | async-start | bytes 1048576 | tf_op jit(solution)/shard_map/all_to_all | solution.py:34
  62.8 1.3 %multiply_reduce_fusion.1 = f32[128]{0:T(128)S(1)} fusion(bf16[32,128,64]{1,2,0:T(8,128)(2,1)} %copy-done.3), kind=kLoop, calls=%fused_computation.26 | loop fusion | flops 786304 | bytes 524800 | tf_op jit(solution)/shard_map/reduce_sum | solution.py:39
  64.6 9.2 %all-to-all-done.3 = bf16[16,8,2048]{2,1,0:T(8,128)(2,1)} async-done(((bf16[16,8,2048]{2,1,0:T(8,128)(2,1)}), bf16[16,8,2048]{2,1,0:T(8,128)(2,1)}, u32[]{:S(2)}, u32[]{:S(2)}) %all-to-all-start.3) | async-done | bytes 524320 | tf_op jit(solution)/shard_map/all_to_all | solution.py:34
  73.7 1.1 convert_reduce_fusion.1
  75.3 0.4 fusion.36
  75.8 0.8 multiply_add_fusion
  76.6 0.4 fusion.34
  77.3 10.0 %all_to_all.42 = bf16[16,8,512]{2,1,0:T(8,128)(2,1)S(1)} all-to-all(bf16[16,8,512]{2,1,0:T(8,128)(2,1)S(1)} %broadcast_in_dim.10), channel_id=1, replica_groups=mesh['dp'=4,'kv'=16,'tp'=2] {'kv'}, dimensions={0} | all-to-all | bytes 262144 | tf_op jit(solution)/shard_map/all_to_all | solution.py:11
  87.3 0.2 convolution_convert_fusion.6
  87.6 5.9 %all_to_all.43 = bf16[2,128,64]{1,2,0:T(8,128)(2,1)S(1)} all-to-all(bf16[2,128,64]{1,2,0:T(8,128)(2,1)S(1)} %bitcast.118), channel_id=1, replica_groups=mesh['dp'=4,'kv'=16,'tp'=2] {'tp'}, dimensions={0} | all-to-all | bytes 65536 | tf_op jit(solution)/shard_map/all_to_all | solution.py:34
  93.6 15.0 %all_to_all.44 = bf16[32,128,64]{1,2,0:T(8,128)(2,1)S(1)} all-to-all(bf16[32,128,64]{1,2,0:T(8,128)(2,1)S(1)} %broadcast_in_dim.11), channel_id=1, replica_groups=mesh['dp'=4,'kv'=16,'tp'=2] {'kv','tp'}, dimensions={0} | all-to-all | bytes 1048576 | tf_op jit(solution)/shard_map/all_to_all | solution.py:11
  108.6 0.3 multiply_reduce_fusion
  108.9 0.3 fusion.7
  109.3 0.3 fusion.51
  109.6 0.7 convolution_convert_fusion
  110.3 0.3 copy.34
  110.6 15.1 %all_to_all.45 = bf16[32,128,64]{1,2,0:T(8,128)(2,1)S(1)} all-to-all(bf16[32,128,64]{1,2,0:T(8,128)(2,1)S(1)} %bitcast.117), channel_id=1, replica_groups=mesh['dp'=4,'kv'=16,'tp'=2] {'kv','tp'}, dimensions={0} | all-to-all | bytes 1048576 | tf_op jit(solution)/shard_map/all_to_all | solution.py:34
  125.7 0.6 add_convert_fusion
  (80 shorter events, 2.7 us)
Async XLA Ops:
  0.6 22.9 %copy-start = (bf16[176,2048]{1,0:T(8,128)(2,1)S(1)}, bf16[176,2048]{1,0:T(8,128)(2,1)}, u32[]{:S(2)}) copy-start(bf16[176,2048]{1,0:T(8,128)(2,1)} %param.26) | copy-start | bytes 2162692
  0.6 22.2 %copy-start.17 = (f32[2048]{0:T(1024)S(1)}, f32[2048]{0:T(1024)}, u32[]{:S(2)}) copy-start(f32[2048]{0:T(1024)} %param.23) | copy-start | bytes 24580
  0.7 22.6 %copy-start.4 = (bf16[2048,176]{0,1:T(8,128)(2,1)S(1)}, bf16[2048,176]{0,1:T(8,128)(2,1)}, u32[]{:S(2)}) copy-start(bf16[2048,176]{0,1:T(8,128)(2,1)} %param.24) | copy-start | bytes 2162692
  1.6 22.0 %copy-start.5 = (bf16[2048,176]{0,1:T(8,128)(2,1)S(1)}, bf16[2048,176]{0,1:T(8,128)(2,1)}, u32[]{:S(2)}) copy-start(bf16[2048,176]{0,1:T(8,128)(2,1)} %param.25) | copy-start | bytes 2162692
  23.6 16.2 %copy-start.14 = (bf16[128,64]{0,1:T(8,128)(2,1)S(1)}, bf16[128,64]{0,1:T(8,128)(2,1)}, u32[]{:S(2)}) copy-start(bf16[128,64]{0,1:T(8,128)(2,1)} %param.22) | copy-start | bytes 49156
  24.3 20.4 %copy-start.22 = (f32[8]{0:T(128)S(1)}, f32[8]{0:T(128)}, u32[]{:S(2)}) copy-start(f32[8]{0:T(128)} %param.35) | copy-start | bytes 100
  24.3 20.5 %copy-start.23 = (f32[8]{0:T(128)S(1)}, f32[8]{0:T(128)}, u32[]{:S(2)}) copy-start(f32[8]{0:T(128)} %param.34) | copy-start | bytes 100
  24.3 31.9 %copy-start.18 = (f32[2048]{0:T(1024)S(1)}, f32[2048]{0:T(1024)}, u32[]{:S(2)}) copy-start(f32[2048]{0:T(1024)} %param.27) | copy-start | bytes 24580
  24.6 31.9 %copy-start.15 = (bf16[2048,8]{0,1:T(8,128)(2,1)S(1)}, bf16[2048,8]{0,1:T(8,128)(2,1)}, u32[]{:S(2)}) copy-start(bf16[2048,8]{0,1:T(8,128)(2,1)} %param.32) | copy-start | bytes 98308
  39.7 17.1 %copy-start.9 = (bf16[128,512]{1,0:T(8,128)(2,1)S(1)}, bf16[128,512]{1,0:T(8,128)(2,1)}, u32[]{:S(2)}) copy-start(bf16[128,512]{1,0:T(8,128)(2,1)} %param.29) | copy-start | bytes 393220
  39.7 17.3 %copy-start.10 = (bf16[128,512]{1,0:T(8,128)(2,1)S(1)}, bf16[128,512]{1,0:T(8,128)(2,1)}, u32[]{:S(2)}) copy-start(bf16[128,512]{1,0:T(8,128)(2,1)} %param.30) | copy-start | bytes 393220
  39.7 17.6 %copy-start.11 = (bf16[128,512]{1,0:T(8,128)(2,1)S(1)}, bf16[128,512]{1,0:T(8,128)(2,1)}, u32[]{:S(2)}) copy-start(bf16[128,512]{1,0:T(8,128)(2,1)} %param.31) | copy-start | bytes 393220
  39.8 17.7 %copy-start.12 = (bf16[128,512]{1,0:T(8,128)(2,1)S(1)}, bf16[128,512]{1,0:T(8,128)(2,1)}, u32[]{:S(2)}) copy-start(bf16[128,512]{1,0:T(8,128)(2,1)} %param.28) | copy-start | bytes 393220
  40.7 15.5 %all-to-all-start.2 = ((bf16[32,128,64]{1,2,0:T(8,128)(2,1)}), bf16[32,128,64]{1,2,0:T(8,128)(2,1)S(1)}, u32[]{:S(2)}, u32[]{:S(2)}) async-start(bf16[32,128,64]{1,2,0:T(8,128)(2,1)} %broadcast_in_dim.9), calls=%async_computation.2 | async-start | bytes 1048576 | tf_op jit(solution)/shard_map/all_to_all | solution.py:11
  56.2 1.3 copy-start.3
  56.5 7.7 %copy-start.16 = (bf16[2048,8]{0,1:T(8,128)(2,1)S(1)}, bf16[2048,8]{0,1:T(8,128)(2,1)}, u32[]{:S(2)}) copy-start(bf16[2048,8]{0,1:T(8,128)(2,1)} %param.33) | copy-start | bytes 98308
  57.0 7.4 %copy-start.20 = (f32[8,4]{0,1:T(4,128)S(1)}, f32[8,4]{0,1:T(4,128)}, u32[]{:S(2)}) copy-start(f32[8,4]{0,1:T(4,128)} %param.36) | copy-start | bytes 388
  57.7 17.6 %copy-start.1 = (f32[8,4,128,128]{3,2,1,0:T(8,128)S(1)}, f32[8,4,128,128]{3,2,1,0:T(8,128)}, u32[]{:S(2)}) copy-start(f32[8,4,128,128]{3,2,1,0:T(8,128)} %param.38) | copy-start | bytes 6291460
  58.5 15.2 %all-to-all-start.3 = ((bf16[16,8,2048]{2,1,0:T(8,128)(2,1)}), bf16[16,8,2048]{2,1,0:T(8,128)(2,1)}, u32[]{:S(2)}, u32[]{:S(2)}) async-start(bf16[16,8,2048]{2,1,0:T(8,128)(2,1)} %pad_maximum_fusion), calls=%async_computation.3 | async-start | bytes 1048576 | tf_op jit(solution)/shard_map/all_to_all | solution.py:34
  76.5 32.1 %copy-start.2 = (f32[8,4,128,128]{3,2,1,0:T(8,128)}, f32[8,4,128,128]{3,2,1,0:T(8,128)S(1)}, u32[]{:S(2)}) copy-start(f32[8,4,128,128]{3,2,1,0:T(8,128)S(1)} %multiply_add_fusion) | copy-start | bytes 6291460
  76.6 0.7 copy-start.21
  76.6 10.8 %copy-start.13 = (bf16[512,128]{1,0:T(8,128)(2,1)S(1)}, bf16[512,128]{1,0:T(8,128)(2,1)}, u32[]{:S(2)}) copy-start(bf16[512,128]{1,0:T(8,128)(2,1)} %param.39) | copy-start | bytes 393220
  76.6 32.3 %copy-start.19 = (f32[2048]{0:T(1024)S(1)}, f32[2048]{0:T(1024)}, u32[]{:S(2)}) copy-start(f32[2048]{0:T(1024)} %param.40) | copy-start | bytes 24580
  77.0 32.3 %copy-start.6 = (bf16[2048,176]{0,1:T(8,128)(2,1)S(1)}, bf16[2048,176]{0,1:T(8,128)(2,1)}, u32[]{:S(2)}) copy-start(bf16[2048,176]{0,1:T(8,128)(2,1)} %param.41) | copy-start | bytes 2162692
  93.6 16.1 %copy-start.7 = (bf16[176,2048]{1,0:T(8,128)(2,1)S(1)}, bf16[176,2048]{1,0:T(8,128)(2,1)}, u32[]{:S(2)}) copy-start(bf16[176,2048]{1,0:T(8,128)(2,1)} %param.43) | copy-start | bytes 2162692
  93.6 16.1 %copy-start.8 = (bf16[2048,176]{0,1:T(8,128)(2,1)S(1)}, bf16[2048,176]{0,1:T(8,128)(2,1)}, u32[]{:S(2)}) copy-start(bf16[2048,176]{0,1:T(8,128)(2,1)} %param.42) | copy-start | bytes 2162692
where the time goes:
time: 127 us; the launch traced here: 126 us
  blocking collectives  82 us (65%)
  waiting for transfers between devices  20.5 us (16%)
  starting transfers between devices  8.18 us (6%)
  other arithmetic  7.21 us (6%)
  matrix products  4.21 us (3%)
  local copies, waits for them, and re-layouts  3.14 us (2%)
    all_to_all x3, blocking collectives, from_everyone(): lax.all_to_all(jnp.broadcast_to(shard[None], (size, *shard.shape)), axis,...  46 us
    all_to_all x3, blocking collectives, sent_and_summed(): tiles = lax.all_to_all(split_up(shard, dim, size), axis, 0, 0, tiled=True)  36 us
    all_to_all x1, waiting for transfers between devices, from_everyone(): lax.all_to_all(jnp.broadcast_to(shard[None], (size, *shard.shape)), axis,...  11.4 us
    all_to_all x1, waiting for transfers between devices, sent_and_summed(): tiles = lax.all_to_all(split_up(shard, dim, size), axis, 0, 0, tiled=True)  9.16 us
    all_to_all x1, starting transfers between devices, sent_and_summed(): tiles = lax.all_to_all(split_up(shard, dim, size), axis, 0, 0, tiled=True)  4.24 us
    all_to_all x1, starting transfers between devices, from_everyone(): lax.all_to_all(jnp.broadcast_to(shard[None], (size, *shard.shape)), axis,...  3.94 us
  transfers between devices with their start and end apart: 2, of which 2 were waited for; matrix products, arithmetic and copies ran while one was open for 2% of the time, Pallas kernels for 0%

commit v1 on v0

v1 whole, which is shorter than its diff:
```python
import jax
import jax.numpy as jnp
from jax import lax
from jax.experimental import pallas as pl
from jax.experimental.pallas import tpu as pltpu
from jax.sharding import PartitionSpec as P

EPS = 1e-06
F32 = jnp.float32
BF16 = jnp.bfloat16
MESH = pl.DeviceIdType.MESH
OFFSETS = sorted(
    [(a, b) for a in (0, 1, 2, 3) for b in (0, 1, 2, 3) if (a, b) != (0, 0)],
    key=lambda o: -(min(o[0], 4 - o[0]) + min(o[1], 4 - o[1])),
)
OWN = 15
ARRIVE = [OWN] + list(range(14, -1, -1))
ARRIVE_GROUPS = [ARRIVE[i : i + 4] for i in range(0, 16, 4)]
SEND_GROUPS = [list(range(i, min(i + 4, 16))) for i in range(0, 16, 4)]


def kernel(
    tok_hbm, g1_hbm, wg1_hbm, wu1_hbm, wd1_hbm, gm_hbm,
    wq_hbm, wk_hbm, wv_hbm, wz_hbm, wstr_hbm, wdec_hbm,
    hdl_hbm, dib_hbm, dex_hbm, hng_hbm, state_hbm, wo_hbm,
    g2_hbm, wg2_hbm, wu2_hbm, wd2_hbm,
    out_ref, key_ref, corr_ref, rate_ref,
    tok, g1, gm, g2, hdl, dib, dex, hng, wstr, wdec,
    wg1, wu1, wd1, wg2, wu2, wd2, wp, wo, state,
    s1, r1, s2, r2, s3, r3, s4, r4, s5, r5, s6, r6, s7, r7,
    rec, sq,
    load_sem, wsend_sem, wrecv_sem,
    ss1, rs1, ss2, rs2, ss3, rs3, ss4, rs4, ss5, rs5, ss6, rs6, ss7, rs7,
):
    me = lax.axis_index("kv")
    c = lax.axis_index("tp")
    z = me // 4
    y = me % 4
    other = 1 - c
    my_half = me // 8

    def chip_to(n):
        a, b = OFFSETS[n] if n != OWN else (0, 0)
        return ((z + a) % 4) * 4 + (y + b) % 4

    def chip_from(n):
        a, b = OFFSETS[n] if n != OWN else (0, 0)
        return ((z + 4 - a) % 4) * 4 + (y + 4 - b) % 4

    def remote(src, dst, send, recv, chip, core):
        return pltpu.make_async_remote_copy(
            src_ref=src, dst_ref=dst, send_sem=send, recv_sem=recv,
            device_id={"kv": chip, "tp": core}, device_id_type=MESH,
        )

    loads = []

    def load(src, dst):
        copy = pltpu.make_async_copy(src, dst, load_sem.at[len(loads)])
        copy.start()
        loads.append(copy)
        return copy

    ld_tok = load(tok_hbm, tok)
    rows_me = pl.ds(pl.multiple_of(me * 128, 128), 128)
    ld_g1 = load(g1_hbm, g1)
    ffn1_src = ((wg1_hbm, wg1), (wu1_hbm, wu1), (wd1_hbm, wd1))
    ffn2_src = ((wg2_hbm, wg2), (wu2_hbm, wu2), (wd2_hbm, wd2))
    ld_ffn1 = [load(src, dst.at[c]) for src, dst in ffn1_src]
    proj_src = (wq_hbm, wk_hbm, wv_hbm, wz_hbm)
    ld_small = [
        load(src, dst)
        for src, dst in (
            (gm_hbm, gm), (g2_hbm, g2), (hdl_hbm, hdl), (dib_hbm, dib), (dex_hbm, dex),
            (hng_hbm, hng), (wstr_hbm.at[rows_me], wstr), (wdec_hbm.at[rows_me], wdec),
        )
    ]
    ld_proj = [
        load(src, wp.at[c, :, pl.ds(512 * m, 512)]) for m, src in enumerate(proj_src)
    ]
    ld_state = load(state_hbm, state)
    ld_wo = load(wo_hbm, wo.at[c])
    ld_ffn2 = [load(src, dst.at[c]) for src, dst in ffn2_src]

    barrier = pltpu.get_barrier_semaphore()
    for n in range(15):
        for t in (0, 1):
            pl.semaphore_signal(
                barrier, inc=1, device_id={"kv": chip_to(n), "tp": t}, device_id_type=MESH
            )
    pl.semaphore_signal(barrier, inc=1, device_id={"kv": me, "tp": other}, device_id_type=MESH)

    ld_tok.wait()
    packed = []
    for t in (0, 1):
        rows = tok[pl.ds(64 * t, 64), :].astype(F32)
        packed.append(jnp.concatenate([rows[:32], rows[32:]], axis=1).astype(BF16))
        s1[t] = packed[t]
    r1[OWN, c] = jnp.where(c == 0, packed[0], packed[1])

    pl.semaphore_wait(barrier, 31)

    sends1 = []
    for n in range(15):
        for t in (0, 1):
            copy = remote(s1.at[t], r1.at[n, c], ss1.at[2 * n + t], rs1.at[2 * n + c], chip_to(n), t)
            copy.start()
            sends1.append(copy)
    own1 = remote(s1.at[other], r1.at[OWN, c], ss1.at[30], rs1.at[30], me, other)
    own1.start()

    wsends = []

    def share(src, dst):
        i = len(wsends)
        copy = remote(src, dst, wsend_sem.at[i], wrecv_sem.at[i], me, other)
        copy.start()
        wsends.append(copy)
        return copy

    sh_ffn1 = [share(src, dst.at[c]) for src, dst in ffn1_src]
    sh_proj = [share(src, wp.at[c, :, pl.ds(512 * m, 512)]) for m, src in enumerate(proj_src)]

    lane = lax.broadcasted_iota(jnp.int32, (32, 128), 1)
    low = lane < 64

    def swap(v):
        return pltpu.roll(v, 64, 1)

    def ffn_hidden(get, gain, w_gate, w_up):
        squares = jnp.zeros((64, 128), F32)
        acc = [[None, None], [None, None]]
        for group in ARRIVE_GROUPS:
            parts, chips = [], []
            for n in group:
                x = get(n)
                j = chip_from(n)
                squares = squares + x * x
                parts.append((x * gain[pl.ds(j, 1), :]).astype(BF16))
                chips.append(j)
            lhs = jnp.concatenate(parts, axis=1)
            for t in (0, 1):
                for k, w in enumerate((w_gate, w_up)):
                    rhs = jnp.concatenate(
                        [w[t, pl.ds(pl.multiple_of(j * 128, 128), 128), :] for j in chips], axis=0
                    )
                    d = jnp.dot(lhs, rhs, preferred_element_type=F32)
                    acc[t][k] = d if acc[t][k] is None else acc[t][k] + d
        scale = lax.rsqrt(jnp.sum(squares, axis=1, keepdims=True) * (1.0 / 2048) + EPS)
        hidden = []
        for t in (0, 1):
            gate = acc[t][0] * scale
            hidden.append((jax.nn.silu(gate) * (acc[t][1] * scale)).astype(BF16))
        return hidden

    def ffn_down(hidden, w_down, emit):
        for group in SEND_GROUPS:
            cols = [pl.ds(pl.multiple_of(chip_to(n) * 128, 128), 128) for n in group]
            total = None
            for t in (0, 1):
                rhs = jnp.concatenate([w_down[t, :, cs] for cs in cols], axis=1)
                d = jnp.dot(hidden[t], rhs, preferred_element_type=F32)
                total = d if total is None else total + d
            for i, n in enumerate(group):
                emit(n, total[:, 128 * i : 128 * (i + 1)])

    own_tokens = []

    def get1(n):
        if n == OWN:
            remote(s1.at[c], r1.at[OWN, other], ss1.at[30], rs1.at[30], me, other).wait_recv()
        else:
            for t in (0, 1):
                remote(s1.at[t], r1.at[n, t], ss1.at[2 * n + t], rs1.at[2 * n + t], me, other).wait_recv()
        b0 = r1[n, 0].astype(F32)
        b1 = r1[n, 1].astype(F32)
        top = jnp.where(low, b0, swap(b1))
        bottom = jnp.where(low, swap(b0), b1)
        x = jnp.concatenate([top, bottom], axis=0)
        if n == OWN:
            own_tokens.append(x)
        return x

    ld_g1.wait()
    for i in (0, 1):
        ld_ffn1[i].wait()
    def shared_wait(i, dst, src):
        remote(src, dst, wsend_sem.at[i], wrecv_sem.at[i], me, other).wait_recv()

    shared_wait(0, wg1.at[other], wg1_hbm)
    shared_wait(1, wu1.at[other], wu1_hbm)
    hidden1 = ffn_hidden(get1, g1, wg1, wu1)

    ld_ffn1[2].wait()
    shared_wait(2, wd1.at[other], wd1_hbm)
    own2 = []
    sends2 = []

    def emit2(n, block):
        if n == OWN:
            own2.append(block)
            return
        s2[n] = block.astype(BF16)
        copy = remote(s2.at[n], r2.at[n], ss2.at[n], rs2.at[n], chip_to(n), c)
        copy.start()
        sends2.append(copy)

    ffn_down(hidden1, wd1, emit2)

    sh_wo = share(wo_hbm, wo.at[c])
    sh_ffn2 = [share(src, dst.at[c]) for src, dst in ffn2_src]

    for ld in ld_small:
        ld.wait()
    for ld in ld_proj:
        ld.wait()
    for m, src in enumerate(proj_src):
        shared_wait(3 + m, wp.at[other, :, pl.ds(512 * m, 512)], src)

    total = own2[0]
    for n in range(14, -1, -1):
        sends2[n].wait_recv()
        total = total + r2[n].astype(F32)
    first = (own_tokens[0] + 0.5 * total).astype(BF16)
    first32 = first.astype(F32)

    scaled = (first32 * gm[pl.ds(me, 1), :]).astype(BF16)
    strength = jnp.dot(scaled, wstr[...], preferred_element_type=F32)
    decay = jnp.dot(scaled, wdec[...], preferred_element_type=F32)
    sum_sq = jnp.sum(first32 * first32, axis=1, keepdims=True)
    extras = jnp.concatenate([strength, decay, sum_sq, jnp.zeros((64, 111), F32)], axis=1)
    extras_hi = extras.astype(BF16).astype(F32)
    extras_lo = extras - extras_hi
    sends3 = []
    for t in (0, 1):
        proj = jnp.dot(scaled, wp[t], preferred_element_type=F32)
        for i in range(8):
            rows = slice(8 * i, 8 * i + 8)
            message = jnp.concatenate(
                [
                    jnp.concatenate([proj[rows, :1024], proj[rows, 1024:]], axis=0),
                    jnp.concatenate([extras_hi[rows], extras_lo[rows]], axis=0),
                ],
                axis=1,
            ).astype(BF16)
            s3[t, i] = message
            target = 8 * c + i
            is_self = jnp.logical_and(target == me, c == t)
            copy = remote(s3.at[t, i], r3.at[me], ss3.at[8 * t + i], rs3.at[me], target, t)
            sends3.append((copy, is_self))

            @pl.when(jnp.logical_not(is_self))
            def _():
                copy.start()

            @pl.when(is_self)
            def _():
                r3[me] = message

    summed = jnp.zeros((16, 1152), F32)
    ld_state.wait()
    for j in range(16):
        is_self = jnp.logical_and(j == me, my_half == c)

        @pl.when(jnp.logical_not(is_self))
        def _():
            remote(s3.at[0, 0], r3.at[j], ss3.at[0], rs3.at[j], me, other).wait_recv()

        summed = summed + r3[j].astype(F32)

    ex = summed[:8, 1024:] + summed[8:, 1024:]
    factor = lax.rsqrt(ex[:, 16:17] * (1.0 / 2048) + EPS)
    ex = ex * factor
    summed = jnp.concatenate([summed[:8, :1024], summed[8:, :1024]], axis=1) * factor
    core0 = c == 0
    queries, keys, values, gates, betas, rates = [], [], [], [], [], []
    for h in range(4):
        def head(m):
            return summed[:, 512 * m + 128 * h : 512 * m + 128 * (h + 1)]

        def unit(u):
            return u * lax.rsqrt(jnp.sum(u * u, axis=1, keepdims=True) + EPS)

        queries.append(unit(jax.nn.silu(head(0))) * 128 ** (-0.5))
        keys.append(unit(jax.nn.silu(head(1))))
        values.append(jax.nn.silu(head(2)))
        gates.append(jax.nn.silu(head(3)))
        betas.append(jax.nn.sigmoid(jnp.where(core0, ex[:, h : h + 1], ex[:, h + 4 : h + 5])))
        decay_in = jnp.where(core0, ex[:, h + 8 : h + 9], ex[:, h + 12 : h + 13])
        bias = jnp.where(core0, dib[:, h : h + 1], dib[:, h + 4 : h + 5])
        log_rate = jnp.where(core0, hdl[:, h : h + 1], hdl[:, h + 4 : h + 5])
        v = decay_in + bias
        softplus = jnp.maximum(v, 0.0) + jnp.log1p(jnp.exp(-jnp.abs(v)))
        rates.append(jnp.exp(dex[:, h : h + 1] - jnp.exp(log_rate) * softplus))
    columns = jnp.concatenate(keys + queries + [jnp.zeros((64, 128), F32)], axis=0).T
    for h in range(4):
        for s in range(8):
            m = 8 * h + s
            block = state[s, h]
            rec[h, pl.ds(s, 1), :] = jnp.sum(block * columns[:, m : m + 1], axis=0, keepdims=True)
            sq[h, pl.ds(s, 1), :] = jnp.sum(
                block * columns[:, 32 + m : 33 + m], axis=0, keepdims=True
            )
    heads = []
    for h in range(4):
        corr = betas[h] * (values[h] - rates[h] * rec[h])
        key_ref[:, h, :] = keys[h]
        corr_ref[:, h, :] = corr
        rate_ref[:, h, :] = jnp.broadcast_to(rates[h], (8, 128))
        key_query = jnp.sum(keys[h] * queries[h], axis=1, keepdims=True)
        read = rates[h] * sq[h] + key_query * corr
        norm = lax.rsqrt(jnp.sum(read * read, axis=1, keepdims=True) * (1.0 / 128) + EPS)
        heads.append(read * norm * hng[...] * gates[h])
    message = jnp.concatenate(
        [jnp.concatenate(heads[:2], axis=1), jnp.concatenate(heads[2:], axis=1)], axis=0
    ).astype(BF16)
    s4[...] = message

    slot = me % 8
    sends4 = []
    for n in range(15):
        copy = remote(
            s4, r4.at[slot, c], ss4.at[n], rs4.at[2 * slot + c], chip_to(n), my_half
        )
        copy.start()
        sends4.append(copy)
    own4 = remote(s4, r4.at[slot, c], ss4.at[OWN], rs4.at[2 * slot + c], me, other)
    stays = c == my_half

    @pl.when(jnp.logical_not(stays))
    def _():
        own4.start()

    @pl.when(stays)
    def _():
        r4[slot, c] = message

    ld_wo.wait()
    shared_wait(7, wo.at[other], wo_hbm)
    mixer = jnp.zeros((64, 128), F32)
    for t in (0, 1):
        rows = []
        for i in range(8):
            is_self = jnp.logical_and(8 * c + i == me, c == t)

            @pl.when(jnp.logical_not(is_self))
            def _():
                remote(s4, r4.at[i, t], ss4.at[0], rs4.at[2 * i + t], me, other).wait_recv()

            part = r4[i, t].astype(F32)
            rows.append(jnp.concatenate([part[:8], part[8:]], axis=1))
        lhs = jnp.concatenate(rows, axis=0).astype(BF16)
        half = jnp.dot(lhs, wo[t], preferred_element_type=F32)
        mixer = mixer + half.astype(BF16).astype(F32)
    second = (first32 + mixer).astype(BF16)
    second32 = second.astype(F32)

    s5[...] = second
    sends5 = []
    for n in range(15):
        copy = remote(s5, r5.at[n], ss5.at[n], rs5.at[n], chip_to(n), c)
        copy.start()
        sends5.append(copy)

    def pack(block):
        upper, lower = block[:32], block[32:]
        return (
            jnp.where(low, upper, swap(lower)).astype(BF16),
            jnp.where(low, swap(upper), lower).astype(BF16),
        )

    p0, p1 = pack(second32)
    s7[0] = p0
    s7[1] = p1
    r7[c] = jnp.where(core0, p0, p1)
    own7 = remote(s7.at[other], r7.at[c], ss7, rs7, me, other)
    own7.start()

    def get5(n):
        if n == OWN:
            return second32
        sends5[n].wait_recv()
        return r5[n].astype(F32)

    for ld in ld_ffn2:
        ld.wait()
    for i, (src, dst) in enumerate(ffn2_src):
        shared_wait(8 + i, dst.at[other], src)
    hidden2 = ffn_hidden(get5, g2, wg2, wu2)

    sends6 = []

    def emit6(n, block):
        packs = pack(block)
        for t in (0, 1):
            s6[n, t] = packs[t]
        if n == OWN:
            r6[OWN, c] = jnp.where(core0, packs[0], packs[1])
            copy = remote(s6.at[OWN, other], r6.at[OWN, c], ss6.at[30], rs6.at[30], me, other)
            copy.start()
            sends6.append(copy)
            return
        for t in (0, 1):
            copy = remote(
                s6.at[n, t], r6.at[n, c], ss6.at[2 * n + t], rs6.at[2 * n + c], chip_to(n), t
            )
            copy.start()
            sends6.append(copy)

    ffn_down(hidden2, wd2, emit6)

    for copy in sends1 + [own1] + wsends + sends2:
        copy.wait_send()
    for copy, is_self in sends3:

        @pl.when(jnp.logical_not(is_self))
        def _():
            copy.wait_send()

    for copy in sends4 + sends5 + [own7]:
        copy.wait_send()

    @pl.when(jnp.logical_not(stays))
    def _():
        own4.wait_send()

    remote(s7.at[0], r7.at[other], ss7, rs7, me, other).wait_recv()
    remote(s6.at[OWN, 0], r6.at[OWN, other], ss6.at[30], rs6.at[30], me, other).wait_recv()
    totals = [r6[OWN, t].astype(F32) for t in (0, 1)]
    for n in range(14, -1, -1):
        for t in (0, 1):
            remote(s6.at[n, t], r6.at[n, t], ss6.at[2 * n + t], rs6.at[2 * n + t], me, other).wait_recv()
            totals[t] = totals[t] + r6[n, t].astype(F32)
    for t in (0, 1):
        value = r7[t].astype(F32) + 0.5 * totals[t]
        out_ref[pl.ds(64 * t, 32), :] = value[:, :64]
        out_ref[pl.ds(64 * t + 32, 32), :] = swap(value)[:, :64]
    for copy in sends6:
        copy.wait_send()


def shards(
    tokens, first_norm_gain, first_gate_weight, first_up_weight, first_down_weight,
    mixer_norm_gain, query_weight, key_weight, value_weight, output_gate_weight,
    strength_weight, decay_weight, head_decay_log, decay_input_bias, decay_extra_log,
    head_norm_gain, state, mixer_output_weight,
    second_norm_gain, second_gate_weight, second_up_weight, second_down_weight,
):
    vm = pltpu.VMEM
    dma = pltpu.SemaphoreType.DMA
    scratch = [
        vm((128, 64), BF16), vm((16, 128), F32), vm((16, 128), F32), vm((16, 128), F32),
        vm((1, 8), F32), vm((1, 8), F32), vm((8, 4), F32), vm((1, 128), F32),
        vm((128, 8), BF16), vm((128, 8), BF16),
        vm((2, 2048, 176), BF16), vm((2, 2048, 176), BF16), vm((2, 176, 2048), BF16),
        vm((2, 2048, 176), BF16), vm((2, 2048, 176), BF16), vm((2, 176, 2048), BF16),
        vm((2, 128, 2048), BF16), vm((2, 512, 128), BF16), vm((8, 4, 128, 128), F32),
        vm((2, 32, 128), BF16), vm((16, 2, 32, 128), BF16),
        vm((15, 64, 128), BF16), vm((15, 64, 128), BF16),
        vm((2, 8, 16, 1152), BF16), vm((16, 16, 1152), BF16),
        vm((16, 256), BF16), vm((8, 2, 16, 256), BF16),
        vm((64, 128), BF16), vm((15, 64, 128), BF16),
        vm((16, 2, 32, 128), BF16), vm((16, 2, 32, 128), BF16),
        vm((2, 32, 128), BF16), vm((2, 32, 128), BF16),
        vm((4, 8, 128), F32), vm((4, 8, 128), F32),
        dma((24,)), dma((11,)), dma((11,)),
        dma((31,)), dma((31,)), dma((15,)), dma((15,)), dma((16,)), dma((16,)),
        dma((16,)), dma((16,)), dma((15,)), dma((15,)), dma((31,)), dma((31,)), dma, dma,
    ]
    small = jax.ShapeDtypeStruct((8, 4, 128), F32)
    out, key_vec, corr, rate = pl.pallas_call(
        kernel,
        out_shape=(jax.ShapeDtypeStruct((128, 64), F32), small, small, small),
        in_specs=[pl.BlockSpec(memory_space=pl.ANY)] * 22,
        out_specs=[pl.BlockSpec(memory_space=pltpu.VMEM)] * 4,
        scratch_shapes=scratch,
        compiler_params=pltpu.CompilerParams(
            collective_id=0, has_side_effects=True, vmem_limit_bytes=40 * 2**20
        ),
        cost_estimate=pl.CostEstimate(
            flops=10**9, bytes_accessed=10**7, transcendentals=10**5
        ),
    )(
        tokens, first_norm_gain.reshape(16, 128), first_gate_weight, first_up_weight,
        first_down_weight, mixer_norm_gain.reshape(16, 128), query_weight, key_weight,
        value_weight, output_gate_weight, strength_weight, decay_weight,
        head_decay_log.reshape(1, 8), decay_input_bias.reshape(1, 8), decay_extra_log,
        head_norm_gain.reshape(1, 128), state, mixer_output_weight,
        second_norm_gain.reshape(16, 128), second_gate_weight, second_up_weight,
        second_down_weight,
    )
    new_state = rate[..., None] * state + key_vec[..., :, None] * corr[..., None, :]
    return (out.astype(BF16), new_state)


def solution(mesh):
    placed = (
        P("dp", ("kv", "tp")), P(), P(None, ("kv", "tp")), P(None, ("kv", "tp")),
        P(("kv", "tp"), None), P(), P("kv", "tp"), P("kv", "tp"), P("kv", "tp"),
        P("kv", "tp"), P(), P(), P(), P(), P(("dp", "kv"), "tp"), P(),
        P(("dp", "kv"), "tp", None, None), P("tp", "kv"), P(), P(None, ("kv", "tp")),
        P(None, ("kv", "tp")), P(("kv", "tp"), None),
    )
    return jax.shard_map(
        shards,
        mesh=mesh,
        in_specs=placed,
        out_specs=(P("dp", ("kv", "tp")), P(("dp", "kv"), "tp", None, None)),
        check_vma=False,
    )
```

time: 127 us -> 88.3 us (0.70)
  blocking collectives: 82 us -> 0 us
  Pallas kernels: 0 us -> 52.8 us
  local copies, waits for them, and re-layouts: 3.14 us -> 30.9 us
  waiting for transfers between devices: 20.5 us -> 0 us
  starting transfers between devices: 8.18 us -> 0 us
  other arithmetic: 7.21 us -> 2.92 us
  matrix products: 4.21 us -> 0 us
    all_to_all x6 -> x0, blocking collectives: 82 us -> none  [the longest x3 46 us: from_everyone(): lax.all_to_all(jnp.broadcast_to(shard[None], (size, *shard.shape)), axis,...]
    pallas_call x0 -> x1, Pallas kernels: none -> 52.8 us  [shards(): pl.pallas_call(kernel, out_shape=(jax.ShapeDtypeStruct((128, 64), F32), s...]
    unnamed x48 -> x57, local copies, waits for them, and re-layouts: 0.3 us -> 30.9 us
    all_to_all x2 -> x0, waiting for transfers between devices: 20.5 us -> none  [the longest x1 11.4 us: from_everyone(): lax.all_to_all(jnp.broadcast_to(shard[None], (size, *shard.shape)), axis,...]
    all_to_all x2 -> x0, starting transfers between devices: 8.18 us -> none  [the longest x1 4.24 us: sent_and_summed(): tiles = lax.all_to_all(split_up(shard, dim, size), axis, 0, 0, tiled=True)]
    dot_general x13 -> x0, matrix products: 4.21 us -> none  [the longest x2 1.32 us: block_terms(): return jnp.dot(hidden, w_down, preferred_element_type=jnp.float32)]
    reduce_sum x9 -> x0, other arithmetic: 3.39 us -> none  [the longest x4 1.99 us: row_scale(): return lax.rsqrt(jnp.mean(values * values, axis=-1, keepdims=True) + EPS)]
    add x1, other arithmetic: 0.76 us -> 2.92 us  [shards(): rate[..., None] * state + key_vec[..., :, None] * corr[..., None, :]]
  transfers between devices with their start and end apart: 2 -> 0, of which waited for: 2 -> 0; matrix products, arithmetic and copies ran while one was open for 2% -> 0% of each run, Pallas kernels for 0% -> 0%
where the time goes in v1:
time: 88.3 us; the launch traced here: 87.3 us
  Pallas kernels  52.8 us (60%)
  local copies, waits for them, and re-layouts  30.9 us (35%)
  other arithmetic  2.92 us (3%)
    pallas_call x1, Pallas kernels, shards(): pl.pallas_call(kernel, out_shape=(jax.ShapeDtypeStruct((128, 64), F32), s...  52.8 us
    unnamed x57, local copies, waits for them, and re-layouts  30.9 us
    add x1, other arithmetic, shards(): rate[..., None] * state + key_vec[..., :, None] * corr[..., None, :]  2.92 us

profile of v1, /device:TPU:1, one launch (start us, length us, event | category | flops | bytes accessed | tf_op | source)
XLA Modules:
  0.0 87.3 jit_solution(14093595273864241592)
XLA Ops:
  0.6 0.0 copy-start.23
  0.6 1.4 %copy.29.dex_hbm = f32[8,4]{1,0:T(8,128)} copy(f32[8,4]{0,1:T(4,128)} %param.36) | data formatting | bytes 256 | tf_op args[14]
  2.1 1.4 %copy.24.tok_hbm = bf16[128,64]{1,0:T(8,128)(2,1)} copy(bf16[128,64]{0,1:T(8,128)(2,1)} %param.22) | data formatting | bytes 32768 | tf_op args[0]
  3.5 1.8 %copy.27.wstr_hbm = bf16[2048,8]{1,0:T(8,128)(2,1)} copy(bf16[2048,8]{0,1:T(8,128)(2,1)} %param.32) | data formatting | bytes 65536 | tf_op args[10]
  5.3 1.8 %copy.28.wdec_hbm = bf16[2048,8]{1,0:T(8,128)(2,1)} copy(bf16[2048,8]{0,1:T(8,128)(2,1)} %param.33) | data formatting | bytes 65536 | tf_op args[11]
  7.0 1.4 %copy.25.wg1_hbm = bf16[2048,176]{1,0:T(8,128)(2,1)S(1)} copy(bf16[2048,176]{0,1:T(8,128)(2,1)} %param.24) | data formatting | bytes 1441792 | tf_op args[2]
  8.5 1.3 %copy.26.wu1_hbm = bf16[2048,176]{1,0:T(8,128)(2,1)} copy(bf16[2048,176]{0,1:T(8,128)(2,1)S(1)} %copy-done.23) | data formatting | bytes 1441792 | tf_op args[3]
  9.8 2.4 %copy.30.wg2_hbm = bf16[2048,176]{1,0:T(8,128)(2,1)} copy(bf16[2048,176]{0,1:T(8,128)(2,1)} %param.41) | data formatting | bytes 1441792 | tf_op args[19]
  12.1 2.2 %copy.31.wu2_hbm = bf16[2048,176]{1,0:T(8,128)(2,1)} copy(bf16[2048,176]{0,1:T(8,128)(2,1)} %param.42) | data formatting | bytes 1441792 | tf_op args[20]
  14.4 0.0 copy-start.1
  14.4 1.2 %copy-done.1 = bf16[2048,176]{1,0:T(8,128)(2,1)S(1)} copy-done((bf16[2048,176]{1,0:T(8,128)(2,1)S(1)}, bf16[2048,176]{1,0:T(8,128)(2,1)}, u32[]{:S(2)}) %copy-start.1) | copy-done | bytes 720920
  15.6 1.2 %copy-done.2 = bf16[2048,176]{1,0:T(8,128)(2,1)S(1)} copy-done((bf16[2048,176]{1,0:T(8,128)(2,1)S(1)}, bf16[2048,176]{1,0:T(8,128)(2,1)}, u32[]{:S(2)}) %copy-start.2) | copy-done | bytes 720920
  16.8 1.2 %copy-done.3 = bf16[2048,176]{1,0:T(8,128)(2,1)S(1)} copy-done((bf16[2048,176]{1,0:T(8,128)(2,1)S(1)}, bf16[2048,176]{1,0:T(8,128)(2,1)}, u32[]{:S(2)}) %copy-start.3) | copy-done | bytes 720920
  18.1 1.0 %copy-done.4 = bf16[2048,8]{1,0:T(8,128)(2,1)S(1)} copy-done((bf16[2048,8]{1,0:T(8,128)(2,1)S(1)}, bf16[2048,8]{1,0:T(8,128)(2,1)}, u32[]{:S(2)}) %copy-start.4) | copy-done | bytes 32792
  19.1 1.0 %copy-done.5 = bf16[2048,8]{1,0:T(8,128)(2,1)S(1)} copy-done((bf16[2048,8]{1,0:T(8,128)(2,1)S(1)}, bf16[2048,8]{1,0:T(8,128)(2,1)}, u32[]{:S(2)}) %copy-start.5) | copy-done | bytes 32792
  20.1 1.1 %copy-done.6 = bf16[176,2048]{1,0:T(8,128)(2,1)S(1)} copy-done((bf16[176,2048]{1,0:T(8,128)(2,1)S(1)}, bf16[176,2048]{1,0:T(8,128)(2,1)}, u32[]{:S(2)}) %copy-start.6) | copy-done | bytes 720920
  21.2 1.1 %copy-done.7 = bf16[176,2048]{1,0:T(8,128)(2,1)S(1)} copy-done((bf16[176,2048]{1,0:T(8,128)(2,1)S(1)}, bf16[176,2048]{1,0:T(8,128)(2,1)}, u32[]{:S(2)}) %copy-start.7) | copy-done | bytes 720920
  22.4 0.9 %copy-done.11 = bf16[128,512]{1,0:T(8,128)(2,1)S(1)} copy-done((bf16[128,512]{1,0:T(8,128)(2,1)S(1)}, bf16[128,512]{1,0:T(8,128)(2,1)}, u32[]{:S(2)}) %copy-start.11) | copy-done | bytes 131096
  23.3 0.9 %copy-done.12 = bf16[512,128]{1,0:T(8,128)(2,1)S(1)} copy-done((bf16[512,128]{1,0:T(8,128)(2,1)S(1)}, bf16[512,128]{1,0:T(8,128)(2,1)}, u32[]{:S(2)}) %copy-start.12) | copy-done | bytes 131096
  24.2 0.8 copy-done.13
  24.9 0.7 copy-done.16
  25.6 0.7 copy-done.17
  26.3 0.7 copy-done.18
  27.0 0.7 copy-done.19
  27.7 0.7 copy-done.20
  28.4 0.7 copy-done.21
  29.0 0.7 copy-done.22
  29.7 52.8 %shard_map.221 = (f32[128,64]{1,0:T(8,128)S(1)}, f32[8,4,128]{2,1,0:T(4,128)S(1)}, f32[8,4,128]{2,1,0:T(4,128)S(1)}, f32[8,4,128]{2,1,0:T(4,128)S(1)}) custom-call(bf16[128,64]{1,0:T(8,128)(2,1)S(1)} %copy-done.13, f32[16,128]{1,0:T(8,128)S(1)} %bitcast.6, bf16[2048,176]{1,0:T(8,128)(2,1)S(1)} %copy.25.wg1_hbm, bf16[2048,176]{1,0:T(8,128)(2,1)S(1)} %copy-done.1, ...), custom_call_target="tpu_custom_call" | custom-call | flops 1000000000 | bytes 10000000 | tf_op jit(solution)/shard_map/pallas_call | solution.py:471
  82.5 0.6 copy-done.14
  83.1 0.6 copy-done.15
  83.7 0.7 copy.32
  84.4 2.9 %multiply_add_fusion = f32[8,4,128,128]{3,2,1,0:T(8,128)} fusion(f32[8,4,128,128]{3,2,1,0:T(8,128)S(1)} %copy-done, f32[8,4,128]{2,1,0:T(4,128)} %copy-done.14, f32[8,4,128]{2,1,0:T(4,128)S(1)} %get-tuple-element.8, f32[8,4,128]{2,1,0:T(4,128)} %copy-done.15), kind=kLoop, calls=%fused_computation | loop fusion | flops 1572864 | bytes 4243456 | tf_op jit(solution)/shard_map/add | solution.py:492
  (28 shorter events, 0.1 us)
Async XLA Ops:
  0.6 7.8 %copy-start.23 = (bf16[2048,176]{0,1:T(8,128)(2,1)S(1)}, bf16[2048,176]{0,1:T(8,128)(2,1)}, u32[]{:S(2)}) copy-start(bf16[2048,176]{0,1:T(8,128)(2,1)} %param.25) | copy-start | bytes 2162692
  9.8 4.6 %copy-start = (f32[8,4,128,128]{3,2,1,0:T(8,128)S(1)}, f32[8,4,128,128]{3,2,1,0:T(8,128)}, u32[]{:S(2)}) copy-start(f32[8,4,128,128]{3,2,1,0:T(8,128)} %state_hbm.1) | copy-start | bytes 6291460
  9.8 4.6 %copy-start.8 = (bf16[128,512]{1,0:T(8,128)(2,1)S(1)}, bf16[128,512]{1,0:T(8,128)(2,1)}, u32[]{:S(2)}) copy-start(bf16[128,512]{1,0:T(8,128)(2,1)} %wq_hbm.1) | copy-start | bytes 393220
  9.8 4.6 %copy-start.9 = (bf16[128,512]{1,0:T(8,128)(2,1)S(1)}, bf16[128,512]{1,0:T(8,128)(2,1)}, u32[]{:S(2)}) copy-start(bf16[128,512]{1,0:T(8,128)(2,1)} %wk_hbm.1) | copy-start | bytes 393220
  9.8 4.6 %copy-start.10 = (bf16[128,512]{1,0:T(8,128)(2,1)S(1)}, bf16[128,512]{1,0:T(8,128)(2,1)}, u32[]{:S(2)}) copy-start(bf16[128,512]{1,0:T(8,128)(2,1)} %wv_hbm.1) | copy-start | bytes 393220
  14.4 1.2 %copy-start.1 = (bf16[2048,176]{1,0:T(8,128)(2,1)S(1)}, bf16[2048,176]{1,0:T(8,128)(2,1)}, u32[]{:S(2)}) copy-start(bf16[2048,176]{1,0:T(8,128)(2,1)} %copy.26.wu1_hbm) | copy-start | bytes 2162692
  15.6 1.2 %copy-start.2 = (bf16[2048,176]{1,0:T(8,128)(2,1)S(1)}, bf16[2048,176]{1,0:T(8,128)(2,1)}, u32[]{:S(2)}) copy-start(bf16[2048,176]{1,0:T(8,128)(2,1)} %copy.30.wg2_hbm) | copy-start | bytes 2162692
  16.8 1.2 %copy-start.3 = (bf16[2048,176]{1,0:T(8,128)(2,1)S(1)}, bf16[2048,176]{1,0:T(8,128)(2,1)}, u32[]{:S(2)}) copy-start(bf16[2048,176]{1,0:T(8,128)(2,1)} %copy.31.wu2_hbm) | copy-start | bytes 2162692
  18.1 1.0 %copy-start.4 = (bf16[2048,8]{1,0:T(8,128)(2,1)S(1)}, bf16[2048,8]{1,0:T(8,128)(2,1)}, u32[]{:S(2)}) copy-start(bf16[2048,8]{1,0:T(8,128)(2,1)} %copy.27.wstr_hbm) | copy-start | bytes 98308
  19.1 1.0 %copy-start.5 = (bf16[2048,8]{1,0:T(8,128)(2,1)S(1)}, bf16[2048,8]{1,0:T(8,128)(2,1)}, u32[]{:S(2)}) copy-start(bf16[2048,8]{1,0:T(8,128)(2,1)} %copy.28.wdec_hbm) | copy-start | bytes 98308
  20.1 1.1 %copy-start.6 = (bf16[176,2048]{1,0:T(8,128)(2,1)S(1)}, bf16[176,2048]{1,0:T(8,128)(2,1)}, u32[]{:S(2)}) copy-start(bf16[176,2048]{1,0:T(8,128)(2,1)} %wd1_hbm.1) | copy-start | bytes 2162692
  21.2 1.1 %copy-start.7 = (bf16[176,2048]{1,0:T(8,128)(2,1)S(1)}, bf16[176,2048]{1,0:T(8,128)(2,1)}, u32[]{:S(2)}) copy-start(bf16[176,2048]{1,0:T(8,128)(2,1)} %wd2_hbm.1) | copy-start | bytes 2162692
  22.4 0.9 %copy-start.11 = (bf16[128,512]{1,0:T(8,128)(2,1)S(1)}, bf16[128,512]{1,0:T(8,128)(2,1)}, u32[]{:S(2)}) copy-start(bf16[128,512]{1,0:T(8,128)(2,1)} %wz_hbm.1) | copy-start | bytes 393220
  23.3 0.9 %copy-start.12 = (bf16[512,128]{1,0:T(8,128)(2,1)S(1)}, bf16[512,128]{1,0:T(8,128)(2,1)}, u32[]{:S(2)}) copy-start(bf16[512,128]{1,0:T(8,128)(2,1)} %wo_hbm.1) | copy-start | bytes 393220
  24.2 0.8 copy-start.13
  24.9 0.7 copy-start.16
  25.6 0.7 copy-start.17
  26.3 0.7 copy-start.18
  27.0 0.7 copy-start.19
  27.7 0.7 copy-start.20
  28.4 0.7 copy-start.21
  29.0 0.7 copy-start.22
  82.5 0.6 copy-start.14
  83.1 0.6 copy-start.15

commit v2 on v1

v2 whole, which is shorter than its diff:
```python
import jax
import jax.numpy as jnp
from jax import lax
from jax.experimental import pallas as pl
from jax.experimental.pallas import tpu as pltpu
from jax.sharding import PartitionSpec as P

EPS = 1e-06
F32 = jnp.float32
BF16 = jnp.bfloat16
MESH = pl.DeviceIdType.MESH
OFFSETS = sorted(
    [(a, b) for a in (0, 1, 2, 3) for b in (0, 1, 2, 3) if (a, b) != (0, 0)],
    key=lambda o: -(min(o[0], 4 - o[0]) + min(o[1], 4 - o[1])),
)
OWN = 15
ARRIVE = [OWN] + list(range(14, -1, -1))
ARRIVE_GROUPS = [ARRIVE[i : i + 4] for i in range(0, 16, 4)]


def group_of(n):
    return 0 if n == OWN else 3 - n // 4


def group_slots(g):
    return pl.ds(12, 3) if g == 0 else pl.ds(12 - 4 * g, 4)


SEND_GROUPS = [list(range(i, min(i + 4, 16))) for i in range(0, 16, 4)]


def kernel(
    tok_hbm, g1_hbm, wg1_hbm, wu1_hbm, wd1_hbm, gm_hbm,
    wq_hbm, wk_hbm, wv_hbm, wz_hbm, wstr_hbm, wdec_hbm,
    hdl_hbm, dib_hbm, dex_hbm, hng_hbm, state_hbm, wo_hbm,
    g2_hbm, wg2_hbm, wu2_hbm, wd2_hbm,
    out_ref, new_ref,
    tok, g1, gm, g2, hdl, dib, dex, hng, wstr, wdec,
    w1, wd1, w2, wd2, wp, wo, state,
    s1, r1, s2, r2, s3, r3, s4, r4, s5, r5, s6, r6, s7, r7,
    rec, sq,
    load_sem, wsend_sem, wrecv_sem,
    ss1, rs1, ss2, rs2, ss3, rs3, ss4, rs4, ss5, rs5, ss6, rs6, sp, rp,
):
    me = lax.axis_index("kv")
    c = lax.axis_index("tp")
    z = me // 4
    y = me % 4
    other = 1 - c
    my_half = me // 8

    def chip_to(n):
        a, b = OFFSETS[n] if n != OWN else (0, 0)
        return ((z + a) % 4) * 4 + (y + b) % 4

    def chip_from(n):
        a, b = OFFSETS[n] if n != OWN else (0, 0)
        return ((z + 4 - a) % 4) * 4 + (y + 4 - b) % 4

    def remote(src, dst, send, recv, chip, core):
        return pltpu.make_async_remote_copy(
            src_ref=src, dst_ref=dst, send_sem=send, recv_sem=recv,
            device_id={"kv": chip, "tp": core}, device_id_type=MESH,
        )

    def load(i, *pairs):
        for src, dst in pairs:
            pltpu.make_async_copy(src, dst, load_sem.at[i]).start()

    def loaded(i, ref):
        pltpu.make_async_copy(ref, ref, load_sem.at[i]).wait()

    rows_me = pl.ds(pl.multiple_of(me * 128, 128), 128)
    proj_src = (wq_hbm, wk_hbm, wv_hbm, wz_hbm)
    first_pairs = ((wg1_hbm, w1.at[c, 0]), (wu1_hbm, w1.at[c, 1]))
    second_pairs = ((wg2_hbm, w2.at[c, 0]), (wu2_hbm, w2.at[c, 1]))
    proj_pairs = tuple(
        (src, wp.at[c, :, pl.ds(512 * m, 512)]) for m, src in enumerate(proj_src)
    )
    load(0, (tok_hbm, tok))
    load(1, (g1_hbm, g1))
    load(2, *first_pairs)
    load(3, (wd1_hbm, wd1.at[c]))
    small_pairs = (
        (gm_hbm, gm), (g2_hbm, g2), (hdl_hbm, hdl), (dib_hbm, dib), (dex_hbm, dex),
        (hng_hbm, hng), (wstr_hbm.at[:, rows_me], wstr), (wdec_hbm.at[:, rows_me], wdec),
    )
    for i, pair in enumerate(small_pairs):
        load(9 + i, pair)
    load(4, *proj_pairs)
    load(5, (state_hbm, state))
    load(6, (wo_hbm, wo.at[c]))
    load(7, *second_pairs)
    load(8, (wd2_hbm, wd2.at[c]))

    barrier = pltpu.get_barrier_semaphore()
    for n in range(15):
        for t in (0, 1):
            pl.semaphore_signal(
                barrier, inc=1, device_id={"kv": chip_to(n), "tp": t}, device_id_type=MESH
            )
    pl.semaphore_signal(barrier, inc=1, device_id={"kv": me, "tp": other}, device_id_type=MESH)

    loaded(0, tok)
    packed = []
    all_rows = tok[...].astype(F32).T
    for t in (0, 1):
        rows = all_rows[64 * t : 64 * t + 64]
        packed.append(jnp.concatenate([rows[:32], rows[32:]], axis=1).astype(BF16))
        s1[t] = packed[t]
    r1[OWN, c] = jnp.where(c == 0, packed[0], packed[1])

    pl.semaphore_wait(barrier, 31)

    for n in range(15):
        for t in (0, 1):
            remote(
                s1.at[t], r1.at[n, c], ss1, rs1.at[group_of(n)], chip_to(n), t
            ).start()
    remote(s1.at[other], r1.at[OWN, c], sp.at[0], rp.at[0], me, other).start()

    def share(i, *pairs):
        for src, dst in pairs:
            remote(src, dst, wsend_sem.at[i], wrecv_sem.at[i], me, other).start()

    def shared(i, ref):
        remote(ref, ref, wsend_sem.at[i], wrecv_sem.at[i], me, other).wait_recv()

    def sent(ref, sem):
        remote(ref, ref, sem, rp.at[0], me, other).wait_send()

    def received(ref, sem):
        remote(ref, ref, sp.at[0], sem, me, other).wait_recv()

    share(0, *first_pairs)
    share(1, (wd1_hbm, wd1.at[c]))
    share(2, *proj_pairs)

    lane = lax.broadcasted_iota(jnp.int32, (32, 128), 1)
    low = lane < 64

    def across(lhs, rhs):
        return lax.dot_general(
            lhs, rhs, (((1,), (1,)), ((), ())), preferred_element_type=F32
        )

    def swap(v):
        return pltpu.roll(v, 64, 1)

    def ffn_hidden(arrived, get, gain, w):
        squares = jnp.zeros((64, 128), F32)
        acc = [[None, None], [None, None]]
        for g, group in enumerate(ARRIVE_GROUPS):
            arrived(g)
            parts, chips = [], []
            for n in group:
                x = get(n)
                j = chip_from(n)
                squares = squares + x * x
                parts.append((x * gain[pl.ds(j, 1), :]).astype(BF16))
                chips.append(j)
            lhs = jnp.concatenate(parts, axis=1)
            for t in (0, 1):
                for k in (0, 1):
                    rhs = jnp.concatenate(
                        [w[t, k, :, pl.ds(pl.multiple_of(j * 128, 128), 128)] for j in chips], axis=1
                    )
                    d = across(lhs, rhs)
                    acc[t][k] = d if acc[t][k] is None else acc[t][k] + d
        scale = lax.rsqrt(jnp.sum(squares, axis=1, keepdims=True) * (1.0 / 2048) + EPS)
        hidden = []
        for t in (0, 1):
            gate = acc[t][0] * scale
            hidden.append((jax.nn.silu(gate) * (acc[t][1] * scale)).astype(BF16))
        return hidden

    def ffn_down(hidden, w_down, emit):
        for group in SEND_GROUPS:
            cols = [pl.ds(pl.multiple_of(chip_to(n) * 128, 128), 128) for n in group]
            total = None
            for t in (0, 1):
                rhs = jnp.concatenate([w_down[t, :, cs] for cs in cols], axis=1)
                d = jnp.dot(hidden[t], rhs, preferred_element_type=F32)
                total = d if total is None else total + d
            for i, n in enumerate(group):
                emit(n, total[:, 128 * i : 128 * (i + 1)])

    own_tokens = []

    def arrived1(g):
        if g == 0:
            received(r1.at[OWN, other], rp.at[0])
        received(r1.at[group_slots(g)], rs1.at[g])

    def get1(n):
        b0 = r1[n, 0].astype(F32)
        b1 = r1[n, 1].astype(F32)
        top = jnp.where(low, b0, swap(b1))
        bottom = jnp.where(low, swap(b0), b1)
        x = jnp.concatenate([top, bottom], axis=0)
        if n == OWN:
            own_tokens.append(x)
        return x

    loaded(1, g1)
    loaded(2, w1.at[c])
    shared(0, w1.at[other])
    hidden1 = ffn_hidden(arrived1, get1, g1, w1)

    loaded(3, wd1.at[c])
    shared(1, wd1.at[other])
    own2 = []

    def emit2(n, block):
        if n == OWN:
            own2.append(block)
            return
        s2[n] = block.astype(BF16)
        remote(s2.at[n], r2.at[n], ss2, rs2.at[n // 8], chip_to(n), c).start()

    ffn_down(hidden1, wd1, emit2)

    share(3, (wo_hbm, wo.at[c]))
    share(4, *second_pairs)
    share(5, (wd2_hbm, wd2.at[c]))

    for i, (_, dst) in enumerate(small_pairs):
        loaded(9 + i, dst)
    loaded(4, wp.at[c])
    shared(2, wp.at[other])

    total = own2[0]
    for n in range(14, -1, -1):
        if n == 14:
            received(r2.at[pl.ds(8, 7)], rs2.at[1])
        if n == 7:
            received(r2.at[pl.ds(0, 8)], rs2.at[0])
        total = total + r2[n].astype(F32)
    first = (own_tokens[0] + 0.5 * total).astype(BF16)
    first32 = first.astype(F32)

    scaled = (first32 * gm[pl.ds(me, 1), :]).astype(BF16)
    strength = across(scaled, wstr[...])
    decay = across(scaled, wdec[...])
    sum_sq = jnp.sum(first32 * first32, axis=1, keepdims=True)
    extras = jnp.concatenate([strength, decay, sum_sq, jnp.zeros((64, 111), F32)], axis=1)
    extras_hi = extras.astype(BF16).astype(F32)
    extras_lo = extras - extras_hi
    for t in (0, 1):
        proj = jnp.dot(scaled, wp[t], preferred_element_type=F32)
        for i in range(8):
            rows = slice(8 * i, 8 * i + 8)
            s3[t, i] = jnp.concatenate(
                [
                    jnp.concatenate([proj[rows, :1024], proj[rows, 1024:]], axis=0),
                    jnp.concatenate([extras_hi[rows], extras_lo[rows]], axis=0),
                ],
                axis=1,
            ).astype(BF16)
        for k in range(8):
            i = (me + 5 + k) % 8
            target = 8 * c + i
            is_self = jnp.logical_and(target == me, c == t)

            @pl.when(jnp.logical_not(is_self))
            def _():
                remote(s3.at[t, i], r3.at[me], ss3, rs3, target, t).start()

            @pl.when(is_self)
            def _():
                r3[me] = s3[t, i]

    loaded(5, state)
    stays = c == my_half

    @pl.when(stays)
    def _():
        received(r3.at[pl.ds(0, 15)], rs3)

    @pl.when(jnp.logical_not(stays))
    def _():
        received(r3, rs3)

    summed = r3[0].astype(F32)
    for j in range(1, 16):
        summed = summed + r3[j].astype(F32)

    ex = summed[:8, 1024:] + summed[8:, 1024:]
    factor = lax.rsqrt(ex[:, 16:17] * (1.0 / 2048) + EPS)
    ex = ex * factor
    summed = jnp.concatenate([summed[:8, :1024], summed[8:, :1024]], axis=1) * factor
    core0 = c == 0
    extra_log = dex[...].T
    queries, keys, values, gates, betas, rates = [], [], [], [], [], []
    for h in range(4):
        def head(m):
            return summed[:, 512 * m + 128 * h : 512 * m + 128 * (h + 1)]

        def unit(u):
            return u * lax.rsqrt(jnp.sum(u * u, axis=1, keepdims=True) + EPS)

        queries.append(unit(jax.nn.silu(head(0))) * 128 ** (-0.5))
        keys.append(unit(jax.nn.silu(head(1))))
        values.append(jax.nn.silu(head(2)))
        gates.append(jax.nn.silu(head(3)))
        betas.append(jax.nn.sigmoid(jnp.where(core0, ex[:, h : h + 1], ex[:, h + 4 : h + 5])))
        decay_in = jnp.where(core0, ex[:, h + 8 : h + 9], ex[:, h + 12 : h + 13])
        bias = jnp.where(core0, dib[:, h : h + 1], dib[:, h + 4 : h + 5])
        log_rate = jnp.where(core0, hdl[:, h : h + 1], hdl[:, h + 4 : h + 5])
        v = decay_in + bias
        softplus = jnp.maximum(v, 0.0) + jnp.log1p(jnp.exp(-jnp.abs(v)))
        rates.append(jnp.exp(extra_log[:, h : h + 1] - jnp.exp(log_rate) * softplus))
    columns = jnp.concatenate(keys + queries + [jnp.zeros((64, 128), F32)], axis=0).T
    for h in range(4):
        for s in range(8):
            m = 8 * h + s
            block = state[s, h]
            rec[h, pl.ds(s, 1), :] = jnp.sum(block * columns[:, m : m + 1], axis=0, keepdims=True)
            sq[h, pl.ds(s, 1), :] = jnp.sum(
                block * columns[:, 32 + m : 33 + m], axis=0, keepdims=True
            )
    heads, corrections = [], []
    for h in range(4):
        corr = betas[h] * (values[h] - rates[h] * rec[h])
        corrections.append(corr)
        key_query = jnp.sum(keys[h] * queries[h], axis=1, keepdims=True)
        read = rates[h] * sq[h] + key_query * corr
        norm = lax.rsqrt(jnp.sum(read * read, axis=1, keepdims=True) * (1.0 / 128) + EPS)
        heads.append(read * norm * hng[...] * gates[h])
    message = jnp.concatenate(
        [jnp.concatenate(heads[:2], axis=1), jnp.concatenate(heads[2:], axis=1)], axis=0
    ).astype(BF16)
    s4[...] = message

    slot = me % 8
    for n in range(15):
        remote(s4, r4.at[c, slot], ss4, rs4.at[c], chip_to(n), my_half).start()

    @pl.when(jnp.logical_not(stays))
    def _():
        remote(s4, r4.at[c, slot], ss4, rs4.at[c], me, other).start()

    @pl.when(stays)
    def _():
        r4[c, slot] = message

    for h in range(4):
        for s in range(8):
            m = 8 * h + s
            new_ref[s, h] = (
                state[s, h] * rates[h][s : s + 1, :]
                + columns[:, m : m + 1] * corrections[h][s : s + 1, :]
            )

    loaded(6, wo.at[c])
    shared(3, wo.at[other])

    @pl.when(stays)
    def _():
        received(r4.at[c, pl.ds(0, 7)], rs4.at[c])

    @pl.when(jnp.logical_not(stays))
    def _():
        received(r4.at[c], rs4.at[c])

    received(r4.at[other], rs4.at[other])
    mixer = jnp.zeros((64, 128), F32)
    for t in (0, 1):
        rows = []
        for i in range(8):
            part = r4[t, i].astype(F32)
            rows.append(jnp.concatenate([part[:8], part[8:]], axis=1))
        lhs = jnp.concatenate(rows, axis=0).astype(BF16)
        half = jnp.dot(lhs, wo[t], preferred_element_type=F32)
        mixer = mixer + half.astype(BF16).astype(F32)
    second = (first32 + mixer).astype(BF16)
    second32 = second.astype(F32)

    s5[...] = second
    for n in range(15):
        remote(s5, r5.at[n], ss5, rs5.at[group_of(n)], chip_to(n), c).start()

    def pack(block):
        upper, lower = block[:32], block[32:]
        return (
            jnp.where(low, upper, swap(lower)).astype(BF16),
            jnp.where(low, swap(upper), lower).astype(BF16),
        )

    p0, p1 = pack(second32)
    s7[0] = p0
    s7[1] = p1
    r7[c] = jnp.where(core0, p0, p1)
    remote(s7.at[other], r7.at[c], sp.at[1], rp.at[1], me, other).start()

    def arrived5(g):
        received(r5.at[group_slots(g)], rs5.at[g])

    def get5(n):
        if n == OWN:
            return second32
        return r5[n].astype(F32)

    loaded(7, w2.at[c])
    shared(4, w2.at[other])
    hidden2 = ffn_hidden(arrived5, get5, g2, w2)
    loaded(8, wd2.at[c])
    shared(5, wd2.at[other])

    def emit6(n, block):
        packs = pack(block)
        for t in (0, 1):
            s6[n, t] = packs[t]
        if n == OWN:
            r6[OWN, c] = jnp.where(core0, packs[0], packs[1])
            remote(s6.at[OWN, other], r6.at[OWN, c], sp.at[2], rp.at[2], me, other).start()
            return
        for t in (0, 1):
            remote(s6.at[n, t], r6.at[n, c], ss6, rs6.at[n // 8], chip_to(n), t).start()

    ffn_down(hidden2, wd2, emit6)

    sent(r1.at[pl.ds(0, 15)], ss1)
    sent(s1.at[0], sp.at[0])
    for i, ref in enumerate((w1, wd1, wp, wo, w2, wd2)):
        sent(ref.at[c], wsend_sem.at[i])
    sent(s2, ss2)

    @pl.when(stays)
    def _():
        sent(r3.at[pl.ds(0, 15)], ss3)
        sent(r6.at[pl.ds(0, 15), 0], ss4)

    @pl.when(jnp.logical_not(stays))
    def _():
        sent(r3, ss3)
        sent(r4, ss4)

    sent(r5, ss5)
    sent(s7.at[0], sp.at[1])

    received(r7.at[other], rp.at[1])
    received(r6.at[OWN, other], rp.at[2])
    totals = [r6[OWN, t].astype(F32) for t in (0, 1)]
    for n in range(14, -1, -1):
        if n == 14:
            received(r6.at[pl.ds(8, 7)], rs6.at[1])
        if n == 7:
            received(r6.at[pl.ds(0, 8)], rs6.at[0])
        for t in (0, 1):
            totals[t] = totals[t] + r6[n, t].astype(F32)
    rows = []
    for t in (0, 1):
        value = r7[t].astype(F32) + 0.5 * totals[t]
        rows += [value, swap(value)]
    out_ref[...] = jnp.concatenate(rows, axis=0).T[:64].astype(BF16)
    sent(r6.at[pl.ds(0, 15)], ss6)
    sent(s6.at[0, 0], sp.at[2])


def shards(
    tokens, first_norm_gain, first_gate_weight, first_up_weight, first_down_weight,
    mixer_norm_gain, query_weight, key_weight, value_weight, output_gate_weight,
    strength_weight, decay_weight, head_decay_log, decay_input_bias, decay_extra_log,
    head_norm_gain, state, mixer_output_weight,
    second_norm_gain, second_gate_weight, second_up_weight, second_down_weight,
):
    vm = pltpu.VMEM
    dma = pltpu.SemaphoreType.DMA
    scratch = [
        vm((64, 128), BF16), vm((16, 128), F32), vm((16, 128), F32), vm((16, 128), F32),
        vm((1, 8), F32), vm((1, 8), F32), vm((4, 8), F32), vm((1, 128), F32),
        vm((8, 128), BF16), vm((8, 128), BF16),
        vm((2, 2, 176, 2048), BF16), vm((2, 176, 2048), BF16),
        vm((2, 2, 176, 2048), BF16), vm((2, 176, 2048), BF16),
        vm((2, 128, 2048), BF16), vm((2, 512, 128), BF16), vm((8, 4, 128, 128), F32),
        vm((2, 32, 128), BF16), vm((16, 2, 32, 128), BF16),
        vm((15, 64, 128), BF16), vm((15, 64, 128), BF16),
        vm((2, 8, 16, 1152), BF16), vm((16, 16, 1152), BF16),
        vm((16, 256), BF16), vm((2, 8, 16, 256), BF16),
        vm((64, 128), BF16), vm((15, 64, 128), BF16),
        vm((16, 2, 32, 128), BF16), vm((16, 2, 32, 128), BF16),
        vm((2, 32, 128), BF16), vm((2, 32, 128), BF16),
        vm((4, 8, 128), F32), vm((4, 8, 128), F32),
        dma((17,)), dma((6,)), dma((6,)),
        dma, dma((4,)), dma, dma((2,)), dma, dma, dma, dma((2,)), dma, dma((4,)), dma, dma((2,)),
        dma((3,)), dma((3,)),
    ]
    out, new_state = pl.pallas_call(
        kernel,
        out_shape=(
            pltpu.VMEM((64, 128), BF16),
            pltpu.VMEM((8, 4, 128, 128), F32),
        ),
        in_specs=[pl.BlockSpec(memory_space=pltpu.HBM)] * 22,
        out_specs=[pl.BlockSpec(memory_space=pltpu.VMEM)] * 2,
        scratch_shapes=scratch,
        compiler_params=pltpu.CompilerParams(
            collective_id=0, has_side_effects=True, vmem_limit_bytes=64900000
        ),
        cost_estimate=pl.CostEstimate(
            flops=10**9, bytes_accessed=10**7, transcendentals=10**5
        ),
    )(
        tokens.T, first_norm_gain.reshape(16, 128), first_gate_weight.T, first_up_weight.T,
        first_down_weight, mixer_norm_gain.reshape(16, 128), query_weight, key_weight,
        value_weight, output_gate_weight, strength_weight.T, decay_weight.T,
        head_decay_log.reshape(1, 8), decay_input_bias.reshape(1, 8), decay_extra_log.T,
        head_norm_gain.reshape(1, 128), state, mixer_output_weight,
        second_norm_gain.reshape(16, 128), second_gate_weight.T, second_up_weight.T,
        second_down_weight,
    )
    return (out.T, new_state)


def solution(mesh):
    placed = (
        P("dp", ("kv", "tp")), P(), P(None, ("kv", "tp")), P(None, ("kv", "tp")),
        P(("kv", "tp"), None), P(), P("kv", "tp"), P("kv", "tp"), P("kv", "tp"),
        P("kv", "tp"), P(), P(), P(), P(), P(("dp", "kv"), "tp"), P(),
        P(("dp", "kv"), "tp", None, None), P("tp", "kv"), P(), P(None, ("kv", "tp")),
        P(None, ("kv", "tp")), P(("kv", "tp"), None),
    )
    return jax.shard_map(
        shards,
        mesh=mesh,
        in_specs=placed,
        out_specs=(P("dp", ("kv", "tp")), P(("dp", "kv"), "tp", None, None)),
        check_vma=False,
    )
```

time: 88.3 us -> 51.9 us (0.59)
  local copies, waits for them, and re-layouts: 30.9 us -> 1.93 us
  Pallas kernels: 52.8 us -> 49.2 us
  other arithmetic: 2.92 us -> 0 us
    unnamed x57 -> x2, local copies, waits for them, and re-layouts: 30.9 us -> 1.93 us
    pallas_call x1, Pallas kernels: 52.8 us -> 49.2 us  [shards(): pl.pallas_call(kernel, out_shape=(pltpu.VMEM((64, 128), BF16), pltpu.VMEM...]
    add x1 -> x0, other arithmetic: 2.92 us -> none  [shards(): rate[..., None] * state + key_vec[..., :, None] * corr[..., None, :]]
where the time goes in v2:
time: 51.9 us; the launch traced here: 51.8 us
  Pallas kernels  49.2 us (95%)
  local copies, waits for them, and re-layouts  1.93 us (4%)
  between operations  0.65 us (1%)
    pallas_call x1, Pallas kernels, shards(): pl.pallas_call(kernel, out_shape=(pltpu.VMEM((64, 128), BF16), pltpu.VMEM...  49.2 us
    unnamed x2, local copies, waits for them, and re-layouts  1.93 us

profile of v2, /device:TPU:1, one launch (start us, length us, event | category | flops | bytes accessed | tf_op | source)
XLA Modules:
  0.0 51.8 jit_solution(9486033050938224175)
XLA Ops:
  0.6 49.2 %shard_map.221 = (bf16[64,128]{1,0:T(8,128)(2,1)S(1)}, f32[8,4,128,128]{3,2,1,0:T(8,128)S(1)}) custom-call(bf16[64,128]{1,0:T(8,128)(2,1)} %bitcast.22, f32[16,128]{1,0:T(8,128)} %bitcast.23, bf16[176,2048]{1,0:T(8,128)(2,1)} %bitcast.16, bf16[176,2048]{1,0:T(8,128)(2,1)} %bitcast.17, bf16[176,2048]{1,0:T(8,128)(2,1)} %wd1_hbm.1, f32[16,128]{1,0:T(8,128)} %bitcast.24, ...), custom_call_target="tpu_custom_call" | custom-call | flops 1000000000 | bytes 10000000 | tf_op jit(solution)/shard_map/pallas_call | solution.py:489
  49.8 0.6 %copy.26 = bf16[128,64]{0,1:T(8,128)(2,1)} copy(bf16[128,64]{0,1:T(8,128)(2,1)S(1)} %bitcast.15) | data formatting | bytes 32768
  50.5 1.3 %copy.27 = f32[8,4,128,128]{3,2,1,0:T(8,128)} copy(f32[8,4,128,128]{3,2,1,0:T(8,128)S(1)} %get-tuple-element.7) | data formatting | bytes 4194304

commit v3 on v2

--- a/solution.py
+++ b/solution.py
@@ -15,15 +15,15 @@
 )
 OWN = 15
 ARRIVE = [OWN] + list(range(14, -1, -1))
-ARRIVE_GROUPS = [ARRIVE[i : i + 4] for i in range(0, 16, 4)]
+ARRIVE_GROUPS = [ARRIVE[i : i + 4] for i in range(12, -1, -4)]
 
 
 def group_of(n):
-    return 0 if n == OWN else 3 - n // 4
+    return 3 if n == OWN else n // 4
 
 
 def group_slots(g):
-    return pl.ds(12, 3) if g == 0 else pl.ds(12 - 4 * g, 4)
+    return pl.ds(12, 3) if g == 3 else pl.ds(4 * g, 4)
 
 
 SEND_GROUPS = [list(range(i, min(i + 4, 16))) for i in range(0, 16, 4)]
@@ -37,10 +37,10 @@
     out_ref, new_ref,
     tok, g1, gm, g2, hdl, dib, dex, hng, wstr, wdec,
     w1, wd1, w2, wd2, wp, wo, state,
-    s1, r1, s2, r2, s3, r3, s4, r4, s5, r5, s6, r6, s7, r7,
+    s1, r1, s2, r2, s3, r3, sx, rx, s4, r4, s5, r5, s6, r6, s7, r7,
     rec, sq,
     load_sem, wsend_sem, wrecv_sem,
-    ss1, rs1, ss2, rs2, ss3, rs3, ss4, rs4, ss5, rs5, ss6, rs6, sp, rp,
+    ss1, rs1, ss2, rs2, ss3, rs3, ssx, rsx, ss4, rs4, ss5, rs5, ss6, rs6, sp, rp,
 ):
     me = lax.axis_index("kv")
     c = lax.axis_index("tp")
@@ -72,15 +72,17 @@
 
     rows_me = pl.ds(pl.multiple_of(me * 128, 128), 128)
     proj_src = (wq_hbm, wk_hbm, wv_hbm, wz_hbm)
-    first_pairs = ((wg1_hbm, w1.at[c, 0]), (wu1_hbm, w1.at[c, 1]))
-    second_pairs = ((wg2_hbm, w2.at[c, 0]), (wu2_hbm, w2.at[c, 1]))
+    rows_c = pl.ds(pl.multiple_of(c * 176, 16), 176)
+    rows_other = pl.ds(pl.multiple_of(other * 176, 16), 176)
+    first_pairs = ((wg1_hbm, w1.at[0, rows_c]), (wu1_hbm, w1.at[1, rows_c]))
+    second_pairs = ((wg2_hbm, w2.at[0, rows_c]), (wu2_hbm, w2.at[1, rows_c]))
     proj_pairs = tuple(
         (src, wp.at[c, :, pl.ds(512 * m, 512)]) for m, src in enumerate(proj_src)
     )
     load(0, (tok_hbm, tok))
     load(1, (g1_hbm, g1))
     load(2, *first_pairs)
-    load(3, (wd1_hbm, wd1.at[c]))
+    load(3, (wd1_hbm, wd1.at[rows_c]))
     small_pairs = (
         (gm_hbm, gm), (g2_hbm, g2), (hdl_hbm, hdl), (dib_hbm, dib), (dex_hbm, dex),
         (hng_hbm, hng), (wstr_hbm.at[:, rows_me], wstr), (wdec_hbm.at[:, rows_me], wdec),
@@ -91,7 +93,7 @@
     load(5, (state_hbm, state))
     load(6, (wo_hbm, wo.at[c]))
     load(7, *second_pairs)
-    load(8, (wd2_hbm, wd2.at[c]))
+    load(8, (wd2_hbm, wd2.at[rows_c]))
 
     barrier = pltpu.get_barrier_semaphore()
     for n in range(15):
@@ -133,7 +135,7 @@
         remote(ref, ref, sp.at[0], sem, me, other).wait_recv()
 
     share(0, *first_pairs)
-    share(1, (wd1_hbm, wd1.at[c]))
+    share(1, (wd1_hbm, wd1.at[rows_c]))
     share(2, *proj_pairs)
 
     lane = lax.broadcasted_iota(jnp.int32, (32, 128), 1)
@@ -149,7 +151,7 @@
 
     def ffn_hidden(arrived, get, gain, w):
         squares = jnp.zeros((64, 128), F32)
-        acc = [[None, None], [None, None]]
+        acc = None
         for g, group in enumerate(ARRIVE_GROUPS):
             arrived(g)
             parts, chips = [], []
@@ -160,35 +162,32 @@
                 parts.append((x * gain[pl.ds(j, 1), :]).astype(BF16))
                 chips.append(j)
             lhs = jnp.concatenate(parts, axis=1)
-            for t in (0, 1):
-                for k in (0, 1):
-                    rhs = jnp.concatenate(
-                        [w[t, k, :, pl.ds(pl.multiple_of(j * 128, 128), 128)] for j in chips], axis=1
-                    )
-                    d = across(lhs, rhs)
-                    acc[t][k] = d if acc[t][k] is None else acc[t][k] + d
+            cols = [pl.ds(pl.multiple_of(j * 128, 128), 128) for j in chips]
+            rhs = jnp.concatenate(
+                [
+                    jnp.concatenate([w[k, :, cs] for k in (0, 1)], axis=0)
+                    for cs in cols
+                ],
+                axis=1,
+            )
+            d = across(lhs, rhs)
+            acc = d if acc is None else acc + d
         scale = lax.rsqrt(jnp.sum(squares, axis=1, keepdims=True) * (1.0 / 2048) + EPS)
-        hidden = []
-        for t in (0, 1):
-            gate = acc[t][0] * scale
-            hidden.append((jax.nn.silu(gate) * (acc[t][1] * scale)).astype(BF16))
-        return hidden
+        gate = acc[:, :352] * scale
+        return (jax.nn.silu(gate) * (acc[:, 352:] * scale)).astype(BF16)
 
     def ffn_down(hidden, w_down, emit):
         for group in SEND_GROUPS:
             cols = [pl.ds(pl.multiple_of(chip_to(n) * 128, 128), 128) for n in group]
-            total = None
-            for t in (0, 1):
-                rhs = jnp.concatenate([w_down[t, :, cs] for cs in cols], axis=1)
-                d = jnp.dot(hidden[t], rhs, preferred_element_type=F32)
-                total = d if total is None else total + d
+            rhs = jnp.concatenate([w_down[:, cs] for cs in cols], axis=1)
+            total = jnp.dot(hidden, rhs, preferred_element_type=F32)
             for i, n in enumerate(group):
                 emit(n, total[:, 128 * i : 128 * (i + 1)])
 
     own_tokens = []
 
     def arrived1(g):
-        if g == 0:
+        if g == 3:
             received(r1.at[OWN, other], rp.at[0])
         received(r1.at[group_slots(g)], rs1.at[g])
 
@@ -203,12 +202,12 @@
         return x
 
     loaded(1, g1)
-    loaded(2, w1.at[c])
-    shared(0, w1.at[other])
+    loaded(2, w1.at[:, rows_c])
+    shared(0, w1.at[:, rows_other])
     hidden1 = ffn_hidden(arrived1, get1, g1, w1)
 
-    loaded(3, wd1.at[c])
-    shared(1, wd1.at[other])
+    loaded(3, wd1.at[rows_c])
+    shared(1, wd1.at[rows_other])
     own2 = []
 
     def emit2(n, block):
@@ -221,8 +220,6 @@
     ffn_down(hidden1, wd1, emit2)
 
     share(3, (wo_hbm, wo.at[c]))
-    share(4, *second_pairs)
-    share(5, (wd2_hbm, wd2.at[c]))
 
     for i, (_, dst) in enumerate(small_pairs):
         loaded(9 + i, dst)
@@ -243,66 +240,84 @@
     strength = across(scaled, wstr[...])
     decay = across(scaled, wdec[...])
     sum_sq = jnp.sum(first32 * first32, axis=1, keepdims=True)
-    extras = jnp.concatenate([strength, decay, sum_sq, jnp.zeros((64, 111), F32)], axis=1)
-    extras_hi = extras.astype(BF16).astype(F32)
-    extras_lo = extras - extras_hi
-    for t in (0, 1):
-        proj = jnp.dot(scaled, wp[t], preferred_element_type=F32)
-        for i in range(8):
-            rows = slice(8 * i, 8 * i + 8)
-            s3[t, i] = jnp.concatenate(
-                [
-                    jnp.concatenate([proj[rows, :1024], proj[rows, 1024:]], axis=0),
-                    jnp.concatenate([extras_hi[rows], extras_lo[rows]], axis=0),
-                ],
-                axis=1,
-            ).astype(BF16)
-        for k in range(8):
-            i = (me + 5 + k) % 8
-            target = 8 * c + i
-            is_self = jnp.logical_and(target == me, c == t)
-
-            @pl.when(jnp.logical_not(is_self))
-            def _():
-                remote(s3.at[t, i], r3.at[me], ss3, rs3, target, t).start()
-
-            @pl.when(is_self)
-            def _():
-                r3[me] = s3[t, i]
+    extras = jnp.concatenate([strength, decay, sum_sq, jnp.zeros((64, 15), F32)], axis=1)
+    extras_hi = extras.astype(BF16)
+    extras_lo = (extras - extras_hi.astype(F32)).astype(BF16)
+    extras = jnp.concatenate([extras_hi, extras_lo, jnp.zeros((64, 64), BF16)], axis=1)
+    for i in range(8):
+        sx[i] = extras[8 * i : 8 * i + 8]
+    stays = c == my_half
+
+    def to_owners(send, source_of, target, recv, own):
+        for t in (0, 1):
+            for k in range(8):
+                i = (me + 5 + k) % 8
+                chip = 8 * c + i
+                is_self = jnp.logical_and(chip == me, c == t)
+
+                @pl.when(jnp.logical_not(is_self))
+                def _():
+                    remote(source_of(t, i), target.at[me], send, recv, chip, t).start()
+
+                @pl.when(is_self)
+                def _():
+                    target[me] = own(t, i)
+
+    def from_owners(ref, sem):
+        @pl.when(stays)
+        def _():
+            received(ref.at[pl.ds(0, 15)], sem)
+
+        @pl.when(jnp.logical_not(stays))
+        def _():
+            received(ref, sem)
+
+    for part in (0, 1):
+        for t in (0, 1):
+            proj = jnp.dot(
+                scaled, wp[t, :, 1024 * part : 1024 * (part + 1)], preferred_element_type=F32
+            )
+            for i in range(8):
+                rows = slice(8 * i, 8 * i + 8)
+                s3[part, t, i] = jnp.concatenate(
+                    [proj[rows, :512], proj[rows, 512:]], axis=0
+                ).astype(BF16)
+        to_owners(
+            ss3.at[part],
+            lambda t, i: s3.at[part, t, i],
+            r3.at[part],
+            rs3.at[part],
+            lambda t, i: s3[part, t, i],
+        )
+        if part == 0:
+            to_owners(ssx, lambda t, i: sx.at[i], rx, rsx, lambda t, i: sx[i])
 
     loaded(5, state)
-    stays = c == my_half
-
-    @pl.when(stays)
-    def _():
-        received(r3.at[pl.ds(0, 15)], rs3)
-
-    @pl.when(jnp.logical_not(stays))
-    def _():
-        received(r3, rs3)
-
-    summed = r3[0].astype(F32)
-    for j in range(1, 16):
-        summed = summed + r3[j].astype(F32)
-
-    ex = summed[:8, 1024:] + summed[8:, 1024:]
+    from_owners(r3.at[0], rs3.at[0])
+    from_owners(rx, rsx)
+
+    def summed_rows(ref):
+        total = ref[0].astype(F32)
+        for j in range(1, 16):
+            total = total + ref[j].astype(F32)
+        return total
+
+    ex = summed_rows(rx)
+    ex = ex + pltpu.roll(ex, 96, 1)
     factor = lax.rsqrt(ex[:, 16:17] * (1.0 / 2048) + EPS)
     ex = ex * factor
-    summed = jnp.concatenate([summed[:8, :1024], summed[8:, :1024]], axis=1) * factor
+    summed = summed_rows(r3.at[0])
     core0 = c == 0
     extra_log = dex[...].T
     queries, keys, values, gates, betas, rates = [], [], [], [], [], []
+
+    def unit(u):
+        return u * lax.rsqrt(jnp.sum(u * u, axis=1, keepdims=True) + EPS)
+
     for h in range(4):
-        def head(m):
-            return summed[:, 512 * m + 128 * h : 512 * m + 128 * (h + 1)]
-
-        def unit(u):
-            return u * lax.rsqrt(jnp.sum(u * u, axis=1, keepdims=True) + EPS)
-
-        queries.append(unit(jax.nn.silu(head(0))) * 128 ** (-0.5))
-        keys.append(unit(jax.nn.silu(head(1))))
-        values.append(jax.nn.silu(head(2)))
-        gates.append(jax.nn.silu(head(3)))
+        lanes = slice(128 * h, 128 * (h + 1))
+        queries.append(unit(jax.nn.silu(summed[:8, lanes] * factor)) * 128 ** (-0.5))
+        keys.append(unit(jax.nn.silu(summed[8:, lanes] * factor)))
         betas.append(jax.nn.sigmoid(jnp.where(core0, ex[:, h : h + 1], ex[:, h + 4 : h + 5])))
         decay_in = jnp.where(core0, ex[:, h + 8 : h + 9], ex[:, h + 12 : h + 13])
         bias = jnp.where(core0, dib[:, h : h + 1], dib[:, h + 4 : h + 5])
@@ -319,6 +334,12 @@
             sq[h, pl.ds(s, 1), :] = jnp.sum(
                 block * columns[:, 32 + m : 33 + m], axis=0, keepdims=True
             )
+    from_owners(r3.at[1], rs3.at[1])
+    summed = summed_rows(r3.at[1])
+    for h in range(4):
+        lanes = slice(128 * h, 128 * (h + 1))
+        values.append(jax.nn.silu(summed[:8, lanes] * factor))
+        gates.append(jax.nn.silu(summed[8:, lanes] * factor))
     heads, corrections = [], []
     for h in range(4):
         corr = betas[h] * (values[h] - rates[h] * rec[h])
@@ -344,6 +365,9 @@
     def _():
         r4[c, slot] = message
 
+    share(4, *second_pairs)
+    share(5, (wd2_hbm, wd2.at[rows_c]))
+
     for h in range(4):
         for s in range(8):
             m = 8 * h + s
@@ -401,11 +425,11 @@
             return second32
         return r5[n].astype(F32)
 
-    loaded(7, w2.at[c])
-    shared(4, w2.at[other])
+    loaded(7, w2.at[:, rows_c])
+    shared(4, w2.at[:, rows_other])
     hidden2 = ffn_hidden(arrived5, get5, g2, w2)
-    loaded(8, wd2.at[c])
-    shared(5, wd2.at[other])
+    loaded(8, wd2.at[rows_c])
+    shared(5, wd2.at[rows_other])
 
     def emit6(n, block):
         packs = pack(block)
@@ -422,18 +446,25 @@
 
     sent(r1.at[pl.ds(0, 15)], ss1)
     sent(s1.at[0], sp.at[0])
-    for i, ref in enumerate((w1, wd1, wp, wo, w2, wd2)):
-        sent(ref.at[c], wsend_sem.at[i])
+    for i, ref in (
+        (0, w1.at[:, rows_c]), (1, wd1.at[rows_c]), (2, wp.at[c]), (3, wo.at[c]),
+        (4, w2.at[:, rows_c]), (5, wd2.at[rows_c]),
+    ):
+        sent(ref, wsend_sem.at[i])
     sent(s2, ss2)
 
     @pl.when(stays)
     def _():
-        sent(r3.at[pl.ds(0, 15)], ss3)
+        for part in (0, 1):
+            sent(r3.at[part, pl.ds(0, 15)], ss3.at[part])
+        sent(rx.at[pl.ds(0, 15)], ssx)
         sent(r6.at[pl.ds(0, 15), 0], ss4)
 
     @pl.when(jnp.logical_not(stays))
     def _():
-        sent(r3, ss3)
+        for part in (0, 1):
+            sent(r3.at[part], ss3.at[part])
+        sent(rx, ssx)
         sent(r4, ss4)
 
     sent(r5, ss5)
@@ -471,19 +502,20 @@
         vm((64, 128), BF16), vm((16, 128), F32), vm((16, 128), F32), vm((16, 128), F32),
         vm((1, 8), F32), vm((1, 8), F32), vm((4, 8), F32), vm((1, 128), F32),
         vm((8, 128), BF16), vm((8, 128), BF16),
-        vm((2, 2, 176, 2048), BF16), vm((2, 176, 2048), BF16),
-        vm((2, 2, 176, 2048), BF16), vm((2, 176, 2048), BF16),
+        vm((2, 352, 2048), BF16), vm((352, 2048), BF16),
+        vm((2, 352, 2048), BF16), vm((352, 2048), BF16),
         vm((2, 128, 2048), BF16), vm((2, 512, 128), BF16), vm((8, 4, 128, 128), F32),
         vm((2, 32, 128), BF16), vm((16, 2, 32, 128), BF16),
         vm((15, 64, 128), BF16), vm((15, 64, 128), BF16),
-        vm((2, 8, 16, 1152), BF16), vm((16, 16, 1152), BF16),
+        vm((2, 2, 8, 16, 512), BF16), vm((2, 16, 16, 512), BF16),
+        vm((8, 8, 128), BF16), vm((16, 8, 128), BF16),
         vm((16, 256), BF16), vm((2, 8, 16, 256), BF16),
         vm((64, 128), BF16), vm((15, 64, 128), BF16),
         vm((16, 2, 32, 128), BF16), vm((16, 2, 32, 128), BF16),
         vm((2, 32, 128), BF16), vm((2, 32, 128), BF16),
         vm((4, 8, 128), F32), vm((4, 8, 128), F32),
         dma((17,)), dma((6,)), dma((6,)),
-        dma, dma((4,)), dma, dma((2,)), dma, dma, dma, dma((2,)), dma, dma((4,)), dma, dma((2,)),
+        dma, dma((4,)), dma, dma((2,)), dma((2,)), dma((2,)), dma, dma, dma, dma((2,)), dma, dma((4,)), dma, dma((2,)),
         dma((3,)), dma((3,)),
     ]
     out, new_state = pl.pallas_call(

time: 51.9 us -> 50.9 us (0.981)
  Pallas kernels: 49.2 us -> 48.1 us
    pallas_call x1, Pallas kernels: 49.2 us -> 48.1 us  [shards(): pl.pallas_call(kernel, out_shape=(pltpu.VMEM((64, 128), BF16), pltpu.VMEM...]
where the time goes in v3:
time: 50.9 us; the launch traced here: 50.7 us
  Pallas kernels  48.1 us (94%)
  local copies, waits for them, and re-layouts  1.93 us (4%)
  between operations  0.65 us (1%)
    pallas_call x1, Pallas kernels, shards(): pl.pallas_call(kernel, out_shape=(pltpu.VMEM((64, 128), BF16), pltpu.VMEM...  48.1 us
    unnamed x2, local copies, waits for them, and re-layouts  1.93 us

profile of v3, /device:TPU:1, one launch (start us, length us, event | category | flops | bytes accessed | tf_op | source)
XLA Modules:
  0.0 50.7 jit_solution(17557450954963773996)
XLA Ops:
  0.6 48.1 %shard_map.221 = (bf16[64,128]{1,0:T(8,128)(2,1)S(1)}, f32[8,4,128,128]{3,2,1,0:T(8,128)S(1)}) custom-call(bf16[64,128]{1,0:T(8,128)(2,1)} %bitcast.22, f32[16,128]{1,0:T(8,128)} %bitcast.23, bf16[176,2048]{1,0:T(8,128)(2,1)} %bitcast.16, bf16[176,2048]{1,0:T(8,128)(2,1)} %bitcast.17, bf16[176,2048]{1,0:T(8,128)(2,1)} %wd1_hbm.1, f32[16,128]{1,0:T(8,128)} %bitcast.24, ...), custom_call_target="tpu_custom_call" | custom-call | flops 1000000000 | bytes 10000000 | tf_op jit(solution)/shard_map/pallas_call | solution.py:521
  48.8 0.6 %copy.26 = bf16[128,64]{0,1:T(8,128)(2,1)} copy(bf16[128,64]{0,1:T(8,128)(2,1)S(1)} %bitcast.15) | data formatting | bytes 32768
  49.4 1.3 %copy.27 = f32[8,4,128,128]{3,2,1,0:T(8,128)} copy(f32[8,4,128,128]{3,2,1,0:T(8,128)S(1)} %get-tuple-element.7) | data formatting | bytes 4194304

commit v4 on v3

--- a/solution.py
+++ b/solution.py
@@ -38,7 +38,7 @@
     tok, g1, gm, g2, hdl, dib, dex, hng, wstr, wdec,
     w1, wd1, w2, wd2, wp, wo, state,
     s1, r1, s2, r2, s3, r3, sx, rx, s4, r4, s5, r5, s6, r6, s7, r7,
-    rec, sq,
+    stack,
     load_sem, wsend_sem, wrecv_sem,
     ss1, rs1, ss2, rs2, ss3, rs3, ssx, rsx, ss4, rs4, ss5, rs5, ss6, rs6, sp, rp,
 ):
@@ -248,20 +248,19 @@
         sx[i] = extras[8 * i : 8 * i + 8]
     stays = c == my_half
 
-    def to_owners(send, source_of, target, recv, own):
-        for t in (0, 1):
-            for k in range(8):
-                i = (me + 5 + k) % 8
-                chip = 8 * c + i
-                is_self = jnp.logical_and(chip == me, c == t)
-
-                @pl.when(jnp.logical_not(is_self))
-                def _():
-                    remote(source_of(t, i), target.at[me], send, recv, chip, t).start()
-
-                @pl.when(is_self)
-                def _():
-                    target[me] = own(t, i)
+    def to_owners(t, send, source_of, target, recv, own):
+        for k in range(8):
+            i = (me + 5 + k) % 8
+            chip = 8 * c + i
+            is_self = jnp.logical_and(chip == me, c == t)
+
+            @pl.when(jnp.logical_not(is_self))
+            def _():
+                remote(source_of(i), target.at[me], send, recv, chip, t).start()
+
+            @pl.when(is_self)
+            def _():
+                target[me] = own(i)
 
     def from_owners(ref, sem):
         @pl.when(stays)
@@ -282,17 +281,24 @@
                 s3[part, t, i] = jnp.concatenate(
                     [proj[rows, :512], proj[rows, 512:]], axis=0
                 ).astype(BF16)
-        to_owners(
-            ss3.at[part],
-            lambda t, i: s3.at[part, t, i],
-            r3.at[part],
-            rs3.at[part],
-            lambda t, i: s3[part, t, i],
-        )
-        if part == 0:
-            to_owners(ssx, lambda t, i: sx.at[i], rx, rsx, lambda t, i: sx[i])
+            to_owners(
+                t,
+                ss3.at[part],
+                lambda i: s3.at[part, t, i],
+                r3.at[part],
+                rs3.at[part],
+                lambda i: s3[part, t, i],
+            )
+            if part == 0:
+                to_owners(t, ssx, lambda i: sx.at[i], rx, rsx, lambda i: sx[i])
 
     loaded(5, state)
+    for h in range(4):
+        for s in range(8):
+            stack[h // 2, 128 * s : 128 * (s + 1), 128 * (h % 2) : 128 * (h % 2 + 1)] = state[
+                s, h
+            ].astype(BF16)
+
     from_owners(r3.at[0], rs3.at[0])
     from_owners(rx, rsx)
 
@@ -325,15 +331,20 @@
         v = decay_in + bias
         softplus = jnp.maximum(v, 0.0) + jnp.log1p(jnp.exp(-jnp.abs(v)))
         rates.append(jnp.exp(extra_log[:, h : h + 1] - jnp.exp(log_rate) * softplus))
-    columns = jnp.concatenate(keys + queries + [jnp.zeros((64, 128), F32)], axis=0).T
-    for h in range(4):
-        for s in range(8):
-            m = 8 * h + s
-            block = state[s, h]
-            rec[h, pl.ds(s, 1), :] = jnp.sum(block * columns[:, m : m + 1], axis=0, keepdims=True)
-            sq[h, pl.ds(s, 1), :] = jnp.sum(
-                block * columns[:, 32 + m : 33 + m], axis=0, keepdims=True
-            )
+    row_seq = lax.broadcasted_iota(jnp.int32, (64, 128), 0) % 8
+    recalls, reads = [], []
+    for pair in (0, 1):
+        rows = keys[2 * pair : 2 * pair + 2] + queries[2 * pair : 2 * pair + 2]
+        rows = jnp.concatenate(rows, axis=0)
+        high = rows.astype(BF16).astype(F32)
+        rows = jnp.concatenate([high, rows - high], axis=0)
+        lhs = jnp.concatenate(
+            [jnp.where(row_seq == s, rows, 0.0) for s in range(8)], axis=1
+        ).astype(BF16)
+        both = jnp.dot(lhs, stack[pair], preferred_element_type=F32)
+        both = both[:32] + both[32:]
+        recalls += [both[:8, :128], both[8:16, 128:]]
+        reads += [both[16:24, :128], both[24:, 128:]]
     from_owners(r3.at[1], rs3.at[1])
     summed = summed_rows(r3.at[1])
     for h in range(4):
@@ -342,10 +353,10 @@
         gates.append(jax.nn.silu(summed[8:, lanes] * factor))
     heads, corrections = [], []
     for h in range(4):
-        corr = betas[h] * (values[h] - rates[h] * rec[h])
+        corr = betas[h] * (values[h] - rates[h] * recalls[h])
         corrections.append(corr)
         key_query = jnp.sum(keys[h] * queries[h], axis=1, keepdims=True)
-        read = rates[h] * sq[h] + key_query * corr
+        read = rates[h] * reads[h] + key_query * corr
         norm = lax.rsqrt(jnp.sum(read * read, axis=1, keepdims=True) * (1.0 / 128) + EPS)
         heads.append(read * norm * hng[...] * gates[h])
     message = jnp.concatenate(
@@ -368,6 +379,7 @@
     share(4, *second_pairs)
     share(5, (wd2_hbm, wd2.at[rows_c]))
 
+    columns = jnp.concatenate(keys + [jnp.zeros((96, 128), F32)], axis=0).T
     for h in range(4):
         for s in range(8):
             m = 8 * h + s
@@ -487,6 +499,15 @@
     out_ref[...] = jnp.concatenate(rows, axis=0).T[:64].astype(BF16)
     sent(r6.at[pl.ds(0, 15)], ss6)
     sent(s6.at[0, 0], sp.at[2])
+
+
+def write_out(out_ref, new_ref, out_hbm, new_hbm, sem):
+    copies = [pltpu.make_async_copy(out_ref, out_hbm, sem.at[8])]
+    copies += [pltpu.make_async_copy(new_ref.at[s], new_hbm.at[s], sem.at[s]) for s in range(8)]
+    for copy in copies:
+        copy.start()
+    for copy in copies:
+        copy.wait()
 
 
 def shards(
@@ -513,7 +534,7 @@
         vm((64, 128), BF16), vm((15, 64, 128), BF16),
         vm((16, 2, 32, 128), BF16), vm((16, 2, 32, 128), BF16),
         vm((2, 32, 128), BF16), vm((2, 32, 128), BF16),
-        vm((4, 8, 128), F32), vm((4, 8, 128), F32),
+        vm((2, 1024, 256), BF16),
         dma((17,)), dma((6,)), dma((6,)),
         dma, dma((4,)), dma, dma((2,)), dma((2,)), dma((2,)), dma, dma, dma, dma((2,)), dma, dma((4,)), dma, dma((2,)),
         dma((3,)), dma((3,)),
@@ -542,6 +563,17 @@
         second_norm_gain.reshape(16, 128), second_gate_weight.T, second_up_weight.T,
         second_down_weight,
     )
+    out, new_state = pl.pallas_call(
+        write_out,
+        out_shape=(
+            jax.ShapeDtypeStruct((64, 128), BF16),
+            jax.ShapeDtypeStruct((8, 4, 128, 128), F32),
+        ),
+        in_specs=[pl.BlockSpec(memory_space=pltpu.VMEM)] * 2,
+        out_specs=[pl.BlockSpec(memory_space=pl.ANY)] * 2,
+        scratch_shapes=[dma((9,))],
+        compiler_params=pltpu.CompilerParams(vmem_limit_bytes=2**22),
+    )(out, new_state)
     return (out.T, new_state)
 
 

time: 50.9 us -> 50 us (0.982)
  local copies, waits for them, and re-layouts: 1.93 us -> 0 us
  Pallas kernels: 48.1 us -> 49.1 us
    unnamed x2 -> x0, local copies, waits for them, and re-layouts: 1.93 us -> none
    pallas_call x0 -> x1, Pallas kernels: none -> 1.39 us  [shards(): pl.pallas_call(write_out, out_shape=(jax.ShapeDtypeStruct((64, 128), BF16...]
where the time goes in v4:
time: 50 us; the launch traced here: 49.8 us
  Pallas kernels  49.1 us (98%)
  between operations  0.65 us (1%)
    pallas_call x1, Pallas kernels, shards(): pl.pallas_call(kernel, out_shape=(pltpu.VMEM((64, 128), BF16), pltpu.VMEM...  47.7 us
    pallas_call x1, Pallas kernels, shards(): pl.pallas_call(write_out, out_shape=(jax.ShapeDtypeStruct((64, 128), BF16...  1.39 us

profile of v4, /device:TPU:1, one launch (start us, length us, event | category | flops | bytes accessed | tf_op | source)
XLA Modules:
  0.0 49.8 jit_solution(15083120349515471825)
XLA Ops:
  0.6 47.7 %shard_map.221 = (bf16[64,128]{1,0:T(8,128)(2,1)S(1)}, f32[8,4,128,128]{3,2,1,0:T(8,128)S(1)}) custom-call(bf16[64,128]{1,0:T(8,128)(2,1)} %bitcast.21, f32[16,128]{1,0:T(8,128)} %bitcast.22, bf16[176,2048]{1,0:T(8,128)(2,1)} %bitcast.15, bf16[176,2048]{1,0:T(8,128)(2,1)} %bitcast.16, bf16[176,2048]{1,0:T(8,128)(2,1)} %wd1_hbm.1, f32[16,128]{1,0:T(8,128)} %bitcast.23, ...), custom_call_target="tpu_custom_call" | custom-call | flops 1000000000 | bytes 10000000 | tf_op jit(solution)/shard_map/pallas_call | solution.py:542
  48.4 1.4 %shard_map.222 = (bf16[64,128]{1,0:T(8,128)(2,1)}, f32[8,4,128,128]{3,2,1,0:T(8,128)}) custom-call(bf16[64,128]{1,0:T(8,128)(2,1)S(1)} %get-tuple-element.6.out_ref, f32[8,4,128,128]{3,2,1,0:T(8,128)S(1)} %get-tuple-element.7.new_ref), custom_call_target="tpu_custom_call" | custom-call | tf_op jit(solution)/shard_map/pallas_call | solution.py:566

commit v5 on v4

--- a/solution.py
+++ b/solution.py
@@ -14,18 +14,6 @@
     key=lambda o: -(min(o[0], 4 - o[0]) + min(o[1], 4 - o[1])),
 )
 OWN = 15
-ARRIVE = [OWN] + list(range(14, -1, -1))
-ARRIVE_GROUPS = [ARRIVE[i : i + 4] for i in range(12, -1, -4)]
-
-
-def group_of(n):
-    return 3 if n == OWN else n // 4
-
-
-def group_slots(g):
-    return pl.ds(12, 3) if g == 3 else pl.ds(4 * g, 4)
-
-
 SEND_GROUPS = [list(range(i, min(i + 4, 16))) for i in range(0, 16, 4)]
 
 
@@ -110,16 +98,16 @@
         rows = all_rows[64 * t : 64 * t + 64]
         packed.append(jnp.concatenate([rows[:32], rows[32:]], axis=1).astype(BF16))
         s1[t] = packed[t]
-    r1[OWN, c] = jnp.where(c == 0, packed[0], packed[1])
+    r1[me, c] = jnp.where(c == 0, packed[0], packed[1])
 
     pl.semaphore_wait(barrier, 31)
 
     for n in range(15):
         for t in (0, 1):
             remote(
-                s1.at[t], r1.at[n, c], ss1, rs1.at[group_of(n)], chip_to(n), t
+                s1.at[t], r1.at[me, c], ss1, rs1.at[z], chip_to(n), t
             ).start()
-    remote(s1.at[other], r1.at[OWN, c], sp.at[0], rp.at[0], me, other).start()
+    remote(s1.at[other], r1.at[me, c], sp.at[0], rp.at[0], me, other).start()
 
     def share(i, *pairs):
         for src, dst in pairs:
@@ -149,27 +137,19 @@
     def swap(v):
         return pltpu.roll(v, 64, 1)
 
-    def ffn_hidden(arrived, get, gain, w):
+    def ffn_hidden(order, arrived, get, gain, w):
         squares = jnp.zeros((64, 128), F32)
         acc = None
-        for g, group in enumerate(ARRIVE_GROUPS):
+        for g in order:
             arrived(g)
-            parts, chips = [], []
-            for n in group:
-                x = get(n)
-                j = chip_from(n)
+            parts = []
+            for j in range(4 * g, 4 * g + 4):
+                x = get(j)
                 squares = squares + x * x
-                parts.append((x * gain[pl.ds(j, 1), :]).astype(BF16))
-                chips.append(j)
+                parts.append((x * gain[j : j + 1, :]).astype(BF16))
             lhs = jnp.concatenate(parts, axis=1)
-            cols = [pl.ds(pl.multiple_of(j * 128, 128), 128) for j in chips]
-            rhs = jnp.concatenate(
-                [
-                    jnp.concatenate([w[k, :, cs] for k in (0, 1)], axis=0)
-                    for cs in cols
-                ],
-                axis=1,
-            )
+            cs = slice(512 * g, 512 * (g + 1))
+            rhs = jnp.concatenate([w[k, :, cs] for k in (0, 1)], axis=0)
             d = across(lhs, rhs)
             acc = d if acc is None else acc + d
         scale = lax.rsqrt(jnp.sum(squares, axis=1, keepdims=True) * (1.0 / 2048) + EPS)
@@ -184,12 +164,17 @@
             for i, n in enumerate(group):
                 emit(n, total[:, 128 * i : 128 * (i + 1)])
 
-    own_tokens = []
+    def from_row(g, ref, sems):
+        @pl.when(z == g)
+        def _():
+            received(ref.at[pl.ds(0, 3)], sems.at[g])
+
+        @pl.when(z != g)
+        def _():
+            received(ref.at[pl.ds(0, 4)], sems.at[g])
 
     def arrived1(g):
-        if g == 3:
-            received(r1.at[OWN, other], rp.at[0])
-        received(r1.at[group_slots(g)], rs1.at[g])
+        from_row(g, r1, rs1)
 
     def get1(n):
         b0 = r1[n, 0].astype(F32)
@@ -197,14 +182,14 @@
         top = jnp.where(low, b0, swap(b1))
         bottom = jnp.where(low, swap(b0), b1)
         x = jnp.concatenate([top, bottom], axis=0)
-        if n == OWN:
-            own_tokens.append(x)
         return x
 
     loaded(1, g1)
     loaded(2, w1.at[:, rows_c])
     shared(0, w1.at[:, rows_other])
-    hidden1 = ffn_hidden(arrived1, get1, g1, w1)
+    received(r1.at[me, other], rp.at[0])
+    hidden1 = ffn_hidden((2, 3, 1, 0), arrived1, get1, g1, w1)
+    own_tokens = get1(me)
 
     loaded(3, wd1.at[rows_c])
     shared(1, wd1.at[rows_other])
@@ -233,7 +218,7 @@
         if n == 7:
             received(r2.at[pl.ds(0, 8)], rs2.at[0])
         total = total + r2[n].astype(F32)
-    first = (own_tokens[0] + 0.5 * total).astype(BF16)
+    first = (own_tokens + 0.5 * total).astype(BF16)
     first32 = first.astype(F32)
 
     scaled = (first32 * gm[pl.ds(me, 1), :]).astype(BF16)
@@ -413,8 +398,9 @@
     second32 = second.astype(F32)
 
     s5[...] = second
+    r5[me] = second
     for n in range(15):
-        remote(s5, r5.at[n], ss5, rs5.at[group_of(n)], chip_to(n), c).start()
+        remote(s5, r5.at[me], ss5, rs5.at[z], chip_to(n), c).start()
 
     def pack(block):
         upper, lower = block[:32], block[32:]
@@ -430,16 +416,14 @@
     remote(s7.at[other], r7.at[c], sp.at[1], rp.at[1], me, other).start()
 
     def arrived5(g):
-        received(r5.at[group_slots(g)], rs5.at[g])
+        from_row(g, r5, rs5)
 
     def get5(n):
-        if n == OWN:
-            return second32
         return r5[n].astype(F32)
 
     loaded(7, w2.at[:, rows_c])
     shared(4, w2.at[:, rows_other])
-    hidden2 = ffn_hidden(arrived5, get5, g2, w2)
+    hidden2 = ffn_hidden((1, 2, 0, 3), arrived5, get5, g2, w2)
     loaded(8, wd2.at[rows_c])
     shared(5, wd2.at[rows_other])
 
@@ -479,7 +463,7 @@
         sent(rx, ssx)
         sent(r4, ss4)
 
-    sent(r5, ss5)
+    sent(r5.at[pl.ds(0, 15)], ss5)
     sent(s7.at[0], sp.at[1])
 
     received(r7.at[other], rp.at[1])
@@ -531,7 +515,7 @@
         vm((2, 2, 8, 16, 512), BF16), vm((2, 16, 16, 512), BF16),
         vm((8, 8, 128), BF16), vm((16, 8, 128), BF16),
         vm((16, 256), BF16), vm((2, 8, 16, 256), BF16),
-        vm((64, 128), BF16), vm((15, 64, 128), BF16),
+        vm((64, 128), BF16), vm((16, 64, 128), BF16),
         vm((16, 2, 32, 128), BF16), vm((16, 2, 32, 128), BF16),
         vm((2, 32, 128), BF16), vm((2, 32, 128), BF16),
         vm((2, 1024, 256), BF16),

time: 50 us -> 49.1 us (0.982)
  Pallas kernels: 49.1 us -> 48.3 us
    pallas_call x1, Pallas kernels: 47.7 us -> 46.9 us  [shards(): pl.pallas_call(kernel, out_shape=(pltpu.VMEM((64, 128), BF16), pltpu.VMEM...]
where the time goes in v5:
time: 49.1 us; the launch traced here: 48.9 us
  Pallas kernels  48.3 us (98%)
  between operations  0.65 us (1%)
    pallas_call x1, Pallas kernels, shards(): pl.pallas_call(kernel, out_shape=(pltpu.VMEM((64, 128), BF16), pltpu.VMEM...  46.9 us
    pallas_call x1, Pallas kernels, shards(): pl.pallas_call(write_out, out_shape=(jax.ShapeDtypeStruct((64, 128), BF16...  1.39 us

profile of v5, /device:TPU:1, one launch (start us, length us, event | category | flops | bytes accessed | tf_op | source)
XLA Modules:
  0.0 48.9 jit_solution(12485093540129237576)
XLA Ops:
  0.6 46.9 %shard_map.221 = (bf16[64,128]{1,0:T(8,128)(2,1)S(1)}, f32[8,4,128,128]{3,2,1,0:T(8,128)S(1)}) custom-call(bf16[64,128]{1,0:T(8,128)(2,1)} %bitcast.21, f32[16,128]{1,0:T(8,128)} %bitcast.22, bf16[176,2048]{1,0:T(8,128)(2,1)} %bitcast.15, bf16[176,2048]{1,0:T(8,128)(2,1)} %bitcast.16, bf16[176,2048]{1,0:T(8,128)(2,1)} %wd1_hbm.1, f32[16,128]{1,0:T(8,128)} %bitcast.23, ...), custom_call_target="tpu_custom_call" | custom-call | flops 1000000000 | bytes 10000000 | tf_op jit(solution)/shard_map/pallas_call | solution.py:526
  47.5 1.4 %shard_map.222 = (bf16[64,128]{1,0:T(8,128)(2,1)}, f32[8,4,128,128]{3,2,1,0:T(8,128)}) custom-call(bf16[64,128]{1,0:T(8,128)(2,1)S(1)} %get-tuple-element.6.out_ref, f32[8,4,128,128]{3,2,1,0:T(8,128)S(1)} %get-tuple-element.7.new_ref), custom_call_target="tpu_custom_call" | custom-call | tf_op jit(solution)/shard_map/pallas_call | solution.py:550

commit v6 on v5

--- a/solution.py
+++ b/solution.py
@@ -440,32 +440,6 @@
 
     ffn_down(hidden2, wd2, emit6)
 
-    sent(r1.at[pl.ds(0, 15)], ss1)
-    sent(s1.at[0], sp.at[0])
-    for i, ref in (
-        (0, w1.at[:, rows_c]), (1, wd1.at[rows_c]), (2, wp.at[c]), (3, wo.at[c]),
-        (4, w2.at[:, rows_c]), (5, wd2.at[rows_c]),
-    ):
-        sent(ref, wsend_sem.at[i])
-    sent(s2, ss2)
-
-    @pl.when(stays)
-    def _():
-        for part in (0, 1):
-            sent(r3.at[part, pl.ds(0, 15)], ss3.at[part])
-        sent(rx.at[pl.ds(0, 15)], ssx)
-        sent(r6.at[pl.ds(0, 15), 0], ss4)
-
-    @pl.when(jnp.logical_not(stays))
-    def _():
-        for part in (0, 1):
-            sent(r3.at[part], ss3.at[part])
-        sent(rx, ssx)
-        sent(r4, ss4)
-
-    sent(r5.at[pl.ds(0, 15)], ss5)
-    sent(s7.at[0], sp.at[1])
-
     received(r7.at[other], rp.at[1])
     received(r6.at[OWN, other], rp.at[2])
     totals = [r6[OWN, t].astype(F32) for t in (0, 1)]
@@ -481,6 +455,32 @@
         value = r7[t].astype(F32) + 0.5 * totals[t]
         rows += [value, swap(value)]
     out_ref[...] = jnp.concatenate(rows, axis=0).T[:64].astype(BF16)
+    sent(r1.at[pl.ds(0, 15)], ss1)
+    sent(s1.at[0], sp.at[0])
+    for i, ref in (
+        (0, w1.at[:, rows_c]), (1, wd1.at[rows_c]), (2, wp.at[c]), (3, wo.at[c]),
+        (4, w2.at[:, rows_c]), (5, wd2.at[rows_c]),
+    ):
+        sent(ref, wsend_sem.at[i])
+    sent(s2, ss2)
+
+    @pl.when(stays)
+    def _():
+        for part in (0, 1):
+            sent(r3.at[part, pl.ds(0, 15)], ss3.at[part])
+        sent(rx.at[pl.ds(0, 15)], ssx)
+        sent(r6.at[pl.ds(0, 15), 0], ss4)
+
+    @pl.when(jnp.logical_not(stays))
+    def _():
+        for part in (0, 1):
+            sent(r3.at[part], ss3.at[part])
+        sent(rx, ssx)
+        sent(r4, ss4)
+
+    sent(r5.at[pl.ds(0, 15)], ss5)
+    sent(s7.at[0], sp.at[1])
+
     sent(r6.at[pl.ds(0, 15)], ss6)
     sent(s6.at[0, 0], sp.at[2])
 

time: 49.1 us -> 49.1 us (level)
  no operation moved by 1% of the time
where the time goes in v6:
time: 49.1 us; the launch traced here: 48.9 us
  Pallas kernels  48.3 us (98%)
  between operations  0.65 us (1%)
    pallas_call x1, Pallas kernels, shards(): pl.pallas_call(kernel, out_shape=(pltpu.VMEM((64, 128), BF16), pltpu.VMEM...  46.9 us
    pallas_call x1, Pallas kernels, shards(): pl.pallas_call(write_out, out_shape=(jax.ShapeDtypeStruct((64, 128), BF16...  1.39 us

profile of v6, /device:TPU:1, one launch (start us, length us, event | category | flops | bytes accessed | tf_op | source)
XLA Modules:
  0.0 48.9 jit_solution(3949148179931269371)
XLA Ops:
  0.6 46.9 %shard_map.221 = (bf16[64,128]{1,0:T(8,128)(2,1)S(1)}, f32[8,4,128,128]{3,2,1,0:T(8,128)S(1)}) custom-call(bf16[64,128]{1,0:T(8,128)(2,1)} %bitcast.21, f32[16,128]{1,0:T(8,128)} %bitcast.22, bf16[176,2048]{1,0:T(8,128)(2,1)} %bitcast.15, bf16[176,2048]{1,0:T(8,128)(2,1)} %bitcast.16, bf16[176,2048]{1,0:T(8,128)(2,1)} %wd1_hbm.1, f32[16,128]{1,0:T(8,128)} %bitcast.23, ...), custom_call_target="tpu_custom_call" | custom-call | flops 1000000000 | bytes 10000000 | tf_op jit(solution)/shard_map/pallas_call | solution.py:526
  47.5 1.4 %shard_map.222 = (bf16[64,128]{1,0:T(8,128)(2,1)}, f32[8,4,128,128]{3,2,1,0:T(8,128)}) custom-call(bf16[64,128]{1,0:T(8,128)(2,1)S(1)} %get-tuple-element.6.out_ref, f32[8,4,128,128]{3,2,1,0:T(8,128)S(1)} %get-tuple-element.7.new_ref), custom_call_target="tpu_custom_call" | custom-call | tf_op jit(solution)/shard_map/pallas_call | solution.py:550

commit v7 on v6

--- a/solution.py
+++ b/solution.py
@@ -51,6 +51,16 @@
             device_id={"kv": chip, "tp": core}, device_id_type=MESH,
         )
 
+    pltpu.make_async_copy(tok_hbm, tok, load_sem.at[0]).start()
+
+    barrier = pltpu.get_barrier_semaphore()
+    for n in range(15):
+        for t in (0, 1):
+            pl.semaphore_signal(
+                barrier, inc=1, device_id={"kv": chip_to(n), "tp": t}, device_id_type=MESH
+            )
+    pl.semaphore_signal(barrier, inc=1, device_id={"kv": me, "tp": other}, device_id_type=MESH)
+
     def load(i, *pairs):
         for src, dst in pairs:
             pltpu.make_async_copy(src, dst, load_sem.at[i]).start()
@@ -67,7 +77,6 @@
     proj_pairs = tuple(
         (src, wp.at[c, :, pl.ds(512 * m, 512)]) for m, src in enumerate(proj_src)
     )
-    load(0, (tok_hbm, tok))
     load(1, (g1_hbm, g1))
     load(2, *first_pairs)
     load(3, (wd1_hbm, wd1.at[rows_c]))
@@ -82,14 +91,6 @@
     load(6, (wo_hbm, wo.at[c]))
     load(7, *second_pairs)
     load(8, (wd2_hbm, wd2.at[rows_c]))
-
-    barrier = pltpu.get_barrier_semaphore()
-    for n in range(15):
-        for t in (0, 1):
-            pl.semaphore_signal(
-                barrier, inc=1, device_id={"kv": chip_to(n), "tp": t}, device_id_type=MESH
-            )
-    pl.semaphore_signal(barrier, inc=1, device_id={"kv": me, "tp": other}, device_id_type=MESH)
 
     loaded(0, tok)
     packed = []
@@ -423,7 +424,7 @@
 
     loaded(7, w2.at[:, rows_c])
     shared(4, w2.at[:, rows_other])
-    hidden2 = ffn_hidden((1, 2, 0, 3), arrived5, get5, g2, w2)
+    hidden2 = ffn_hidden((1, 2, 3, 0), arrived5, get5, g2, w2)
     loaded(8, wd2.at[rows_c])
     shared(5, wd2.at[rows_other])
 

time: 49.1 us -> 49.2 us (level)
  no operation moved by 1% of the time
where the time goes in v7:
time: 49.2 us; the launch traced here: 49 us
  Pallas kernels  48.3 us (98%)
  between operations  0.65 us (1%)
    pallas_call x1, Pallas kernels, shards(): pl.pallas_call(kernel, out_shape=(pltpu.VMEM((64, 128), BF16), pltpu.VMEM...  47 us
    pallas_call x1, Pallas kernels, shards(): pl.pallas_call(write_out, out_shape=(jax.ShapeDtypeStruct((64, 128), BF16...  1.39 us

profile of v7, /device:TPU:1, one launch (start us, length us, event | category | flops | bytes accessed | tf_op | source)
XLA Modules:
  0.0 49.0 jit_solution(1922514717991342055)
XLA Ops:
  0.6 47.0 %shard_map.221 = (bf16[64,128]{1,0:T(8,128)(2,1)S(1)}, f32[8,4,128,128]{3,2,1,0:T(8,128)S(1)}) custom-call(bf16[64,128]{1,0:T(8,128)(2,1)} %bitcast.21, f32[16,128]{1,0:T(8,128)} %bitcast.22, bf16[176,2048]{1,0:T(8,128)(2,1)} %bitcast.15, bf16[176,2048]{1,0:T(8,128)(2,1)} %bitcast.16, bf16[176,2048]{1,0:T(8,128)(2,1)} %wd1_hbm.1, f32[16,128]{1,0:T(8,128)} %bitcast.23, ...), custom_call_target="tpu_custom_call" | custom-call | flops 1000000000 | bytes 10000000 | tf_op jit(solution)/shard_map/pallas_call | solution.py:527
  47.6 1.4 %shard_map.222 = (bf16[64,128]{1,0:T(8,128)(2,1)}, f32[8,4,128,128]{3,2,1,0:T(8,128)}) custom-call(bf16[64,128]{1,0:T(8,128)(2,1)S(1)} %get-tuple-element.6.out_ref, f32[8,4,128,128]{3,2,1,0:T(8,128)S(1)} %get-tuple-element.7.new_ref), custom_call_target="tpu_custom_call" | custom-call | tf_op jit(solution)/shard_map/pallas_call | solution.py:551
